TPU v7x, 128 devices: a whole 4x4x4 slice. The times are simulated.
128 devices in a mesh: sp: 64 (over z, y, x), tp: 2 (over core).
Axes of the slice: x: 4, y: 4, z: 4, core: 2. Of those that a mesh axis runs over, the one named last changes fastest.
Arguments:
- mid_rows: bfloat16 [8192, 2048], P(('sp', 'tp')), may hold values from -6 to 6
- cotangent: bfloat16 [8192, 2048], P(('sp', 'tp')), may hold values from -24 to 24
- route_experts: int32 [8192, 2], P(('sp', 'tp')), may hold values from 0 to 63, as said below
- route_weights: float32 [8192, 2], P(('sp', 'tp')), may hold values from 0.05 to 0.6
- gate_weight: bfloat16 [64, 2048, 1024], P('sp', None, 'tp'), may hold values from -0.125 to 0.125
- up_weight: bfloat16 [64, 2048, 1024], P('sp', None, 'tp'), may hold values from -0.125 to 0.125
- down_weight: bfloat16 [64, 1024, 2048], P('sp', 'tp'), may hold values from -0.1875 to 0.1875
- out_weight: bfloat16 [2048, 2048], P(None, 'tp'), may hold values from -0.125 to 0.125
- queries: bfloat16 [8192, 1024], P('sp', 'tp'), may hold values from -6 to 6
- key_rows: bfloat16 [8192, 1024], P('sp', 'tp'), may hold values from -6 to 6
- value_rows: bfloat16 [8192, 2048], P('sp', 'tp'), may hold values from -6 to 6
- log_decay: float32 [8192, 1024], P('sp', 'tp'), may hold values from -1 to 0
Outputs:
- gate_gradient: bfloat16 [64, 2048, 1024], P('sp', None, 'tp')
- up_gradient: bfloat16 [64, 2048, 1024], P('sp', None, 'tp')
- down_gradient: bfloat16 [64, 1024, 2048], P('sp', 'tp')
- out_gradient: float32 [2048, 2048], P('sp', 'tp')
- query_gradient: bfloat16 [8192, 1024], P('sp', 'tp')
- key_gradient: bfloat16 [8192, 1024], P('sp', 'tp')
- value_gradient: bfloat16 [8192, 2048], P('sp', 'tp')
- decay_gradient: float32 [8192, 1024], P('sp', 'tp')
Inputs may be any that keep to these rules, and one draw needn't show every extreme that they name: `route_experts`: each row names two different experts of one group: both lie among the same 16 consecutive numbers starting at a multiple of 16. Among the rows of one device, no expert is named more than 4 times, and one expert exactly 4 times.
All inputs are finite; a program needn't handle non-finite values.
Results may differ from a plain program's by a relative error of at most 0.0058.
Values may be sent and summed in bfloat16 or wider, within the bound.
No kernel may reach another device: no remote copies, remote signals or barrier semaphores. Data moves between devices by JAX's collectives and lax.ppermute only.
A program may use at most 192 MiB of HBM per device.

v0:
```python
import functools

import jax
import jax.numpy as jnp
from jax import lax
from jax.experimental import pallas as pl
from jax.experimental.pallas import tpu as pltpu
from jax.sharding import Mesh
from jax.sharding import PartitionSpec as P

DK = 128
DV = 256
SP = ("sp_0", "sp_1", "sp_2")
SP_TP = ("sp_0", "sp_1", "sp_2", "tp")
ROWS = 64
D = 2048
HALF = 1024
HID = 512
HEADS = 4
TOK = 128
NDEV = 64
SW = DV + 128
MSG = SW + D
RET = DV + HALF
SCALE = DK**-0.5

f32 = jnp.float32
bf16 = jnp.bfloat16
epsilon = 1e-06


def dot(a, b, ca, cb, high=False):
    return lax.dot_general(
        a,
        b,
        (((ca,), (cb,)), ((), ())),
        precision=lax.Precision.HIGHEST if high else None,
        preferred_element_type=f32,
    )


def call(kernel, out_shape, args, specs=None, scratch=(), flops=0, name=None):
    specs = specs or [None] * len(args)
    vmem = pl.BlockSpec(memory_space=pltpu.VMEM)
    many = isinstance(out_shape, (list, tuple))
    return pl.pallas_call(
        kernel,
        out_shape=out_shape,
        in_specs=[s or vmem for s in specs],
        out_specs=[vmem] * len(out_shape) if many else vmem,
        scratch_shapes=list(scratch),
        compiler_params=pltpu.CompilerParams(vmem_limit_bytes=56 * 1024 * 1024),
        cost_estimate=pl.CostEstimate(flops=flops, transcendentals=0, bytes_accessed=1 << 20),
        name=name,
    )(*args)


SMEM = pl.BlockSpec(memory_space=pltpu.SMEM)
ANY = pl.BlockSpec(memory_space=pl.ANY)


def tri(lower, strict=False):
    i = lax.broadcasted_iota(jnp.int32, (TOK, TOK), 0)
    j = lax.broadcasted_iota(jnp.int32, (TOK, TOK), 1)
    return (i >= j) if lower else (i <= j)


def head_cols(ref, h, width):
    return ref[:, h * width : (h + 1) * width].astype(f32)


def state_kernel(k_ref, v_ref, a_ref, msg_ref):
    lower = tri(True).astype(f32)
    ones = jnp.ones((TOK, 128), f32)
    lane = lax.broadcasted_iota(jnp.int32, (DK, 128), 1)
    for h in range(HEADS):
        a = head_cols(a_ref, h, DK)
        r = dot(lower, a, 1, 0, True)
        ke = head_cols(k_ref, h, DK) * jnp.exp(r[TOK - 1 :, :] - r)
        s = dot(ke, head_cols(v_ref, h, DV), 0, 0, True)
        rows = slice(h * DK, (h + 1) * DK)
        msg_ref[rows, 0:DV] = s.astype(bf16)
        col = dot(a, ones, 0, 0, True)
        hi = col.astype(bf16).astype(f32)
        mid = (col - hi).astype(bf16).astype(f32)
        lo = col - hi - mid
        part = jnp.where(lane == 0, hi, jnp.where(lane == 1, mid, jnp.where(lane == 2, lo, 0.0)))
        msg_ref[rows, DV:SW] = part.astype(bf16)


def pack_kernel(core_ref, route_ref, route2_ref, mid_ref, mid2_ref, cot_ref, cot2_ref, st_ref, out_ref, pick_ref):
    core = core_ref[0]
    lane = lax.broadcasted_iota(jnp.int32, (ROWS, NDEV), 1).astype(f32)
    ti = lax.broadcasted_iota(jnp.int32, (ROWS, ROWS), 0)
    tj = lax.broadcasted_iota(jnp.int32, (ROWS, ROWS), 1)
    before = (ti > tj).astype(f32)
    si = lax.broadcasted_iota(jnp.int32, (8 * NDEV, NDEV), 0)
    se = lax.broadcasted_iota(jnp.int32, (8 * NDEV, NDEV), 1)
    expand = (si // 8 == se).astype(f32)
    slot = (si % 4 + 1).astype(f32)
    owner = (si % 8) // 4

    def picks(ref, which):
        e1 = (ref[:, 0:1] == lane).astype(f32)
        e2 = (ref[:, 1:2] == lane).astype(f32)
        both = e1 + e2
        rank = both * (dot(before, both, 1, 0, True) + 1.0)
        weight = e1 * ref[:, 2:3] + e2 * ref[:, 3:4]
        found = dot(expand, rank, 1, 1, True)
        pick = jnp.where((found == slot) & (owner == which), 1.0, 0.0)
        w = jnp.sum(pick * dot(expand, weight, 1, 1, True), axis=1, keepdims=True)
        return pick, w

    own, w_own = picks(route_ref, core)
    other, w_other = picks(route2_ref, 1 - core)
    pick_ref[:, 0:ROWS] = own.astype(bf16)
    pick_ref[:, ROWS:] = other.astype(bf16)
    out_ref[:, 0:SW] = st_ref[...]
    own = own.astype(bf16)
    other = other.astype(bf16)

    @pl.when(core == 0)
    def _():
        rows = dot(own, mid_ref[...], 1, 0) + dot(other, mid2_ref[...], 1, 0)
        out_ref[:, SW:] = rows.astype(bf16)

    @pl.when(core == 1)
    def _():
        rows = dot(own, cot_ref[...], 1, 0) + dot(other, cot2_ref[...], 1, 0)
        out_ref[:, SW:] = (rows * (w_own + w_other)).astype(bf16)


def scan_kernel(msg_ref, dec_ref, out_ref, x_ref, d_ref, y_ref, *, reverse):
    x_ref[...] = msg_ref[:, 0:DV].astype(f32)
    log = jnp.sum(dec_ref[...].astype(f32), axis=1, keepdims=True)
    d_ref[...] = jnp.broadcast_to(jnp.exp(log), (8 * NDEV, DV))
    state = jnp.zeros((8, DV), f32)
    for n in range(NDEV):
        p = NDEV - 1 - n if reverse else n
        rows = slice(8 * p, 8 * p + 8)
        y_ref[rows, :] = state
        state = d_ref[rows, :] * state + x_ref[rows, :]
    out_ref[...] = y_ref[...].astype(bf16)


def expert_kernel(
    core_ref, mine_ref, theirs_ref, gate_ref, up_ref, down_ref,
    keep_ref, send_ref, rows_ref, scaled_ref, hidden_ref, bg_ref, bu_ref,
    sems,
):
    core = core_ref[0]
    part = (slice(None), pl.ds(SW, D))

    def fetch(a_ref, b_ref):
        first = pltpu.make_async_copy(a_ref.at[part], rows_ref, sems.at[0])
        second = pltpu.make_async_copy(b_ref.at[part], scaled_ref, sems.at[1])
        first.start()
        second.start()
        first.wait()
        second.wait()

    @pl.when(core == 0)
    def _():
        fetch(mine_ref, theirs_ref)

    @pl.when(core == 1)
    def _():
        fetch(theirs_ref, mine_ref)

    x = rows_ref[...]
    pre_gate = dot(x, gate_ref[...], 1, 0)
    pre_up = dot(x, up_ref[...], 1, 0)
    sig = 1.0 / (1.0 + jnp.exp(-pre_gate))
    swish = pre_gate * sig
    slope = sig * (1.0 + pre_gate * (1.0 - sig))
    hidden_ref[...] = (swish * pre_up).astype(bf16)
    back = dot(scaled_ref[...], down_ref[...], 1, 1)
    bg = (back * pre_up * slope).astype(bf16)
    bu = (back * swish).astype(bf16)
    bg_ref[...] = bg
    bu_ref[...] = bu

    def half(c):
        cols = pl.ds(pl.multiple_of(c * HALF, HALF), HALF)
        total = dot(bg, gate_ref[cols, :], 1, 1) + dot(bu, up_ref[cols, :], 1, 1)
        return total.astype(bf16)

    send_ref[...] = half(1 - core)
    keep_ref[...] = half(core)


def return_kernel(keep_ref, got_ref, state_ref, out_ref):
    out_ref[:, 0:DV] = state_ref[...]
    out_ref[:, DV:] = (keep_ref[...].astype(f32) + got_ref[...].astype(f32)).astype(bf16)


def combine_kernel(core_ref, pick_ref, ret_ref, cot_ref, cot2_ref, out_ref):
    core = core_ref[0]
    rows = ret_ref[:, DV:]
    cols = pl.ds(pl.multiple_of(core * HALF, HALF), HALF)

    def put(lanes, cot, which):
        total = dot(pick_ref[:, lanes], rows, 0, 0) + cot[:, cols].astype(f32)
        out_ref[pl.ds(pl.multiple_of(which * ROWS, ROWS), ROWS), :] = total.astype(bf16)

    put(slice(0, ROWS), cot_ref, core)
    put(slice(ROWS, 2 * ROWS), cot2_ref, 1 - core)


def forward_parts(q_ref, k_ref, v_ref, a_ref, h):
    lower = tri(True)
    r = dot(lower.astype(f32), head_cols(a_ref, h, DK), 1, 0, True)
    mid = r[TOK // 2 : TOK // 2 + 1, :]
    up = jnp.exp(r - mid)
    down = jnp.exp(mid - r)
    q = head_cols(q_ref, h, DK) * SCALE
    k = head_cols(k_ref, h, DK)
    v = head_cols(v_ref, h, DV)
    qd = q * up
    ki = k * down
    scores = jnp.where(lower, dot(qd, ki, 1, 1, True), 0.0)
    return r, up, down, q, k, v, qd, ki, scores


def mixer_kernel(
    core_ref, mine_ref, theirs_ref, w_ref, q_ref, k_ref, v_ref, a_ref, ret_ref,
    msg_ref, og_ref, braw_ref,
):
    core = core_ref[0]
    mine = mine_ref[...]
    theirs = theirs_ref[...]
    row_mine = pl.multiple_of(core * HALF, HALF)
    row_theirs = pl.multiple_of((1 - core) * HALF, HALF)
    braw_ref[...] = dot(mine, w_ref[pl.ds(row_mine, HALF), :], 1, 0) + dot(
        theirs, w_ref[pl.ds(row_theirs, HALF), :], 1, 0
    )
    for i in range(2):
        cols = slice(i * HID, (i + 1) * HID)
        og_ref[2 * core + i, :, 0:HID] = mine[:, cols]
        og_ref[2 * (1 - core) + i, :, 0:HID] = theirs[:, cols]
    for h in range(HEADS):
        r, up, down, q, k, v, qd, ki, scores = forward_parts(q_ref, k_ref, v_ref, a_ref, h)
        rows = slice(h * DK, (h + 1) * DK)
        cols = slice(h * DV, (h + 1) * DV)
        s_in = ret_ref[rows, 0:DV].astype(f32)
        q_abs = q * jnp.exp(r)
        raw = dot(scores, v, 1, 0, True) + dot(q_abs, s_in, 1, 0, True)
        inv = lax.rsqrt(jnp.mean(raw * raw, axis=1, keepdims=True) + epsilon)
        normed = raw * inv
        bn = braw_ref[:, cols]
        braw = inv * (bn - normed * jnp.mean(bn * normed, axis=1, keepdims=True))
        braw_ref[:, cols] = braw
        msg_ref[rows, :] = dot(q_abs, braw, 0, 0, True).astype(bf16)
        normed = normed.astype(bf16)
        for z in range(4):
            og_ref[z, :, HID + h * DV : HID + (h + 1) * DV] = normed


def local_kernel(
    q_ref, k_ref, v_ref, a_ref, ret_ref, braw_ref, qo_ref, dk_ref, dv_ref, dd_ref
):
    for h in range(HEADS):
        r, up, down, q, k, v, qd, ki, scores = forward_parts(q_ref, k_ref, v_ref, a_ref, h)
        rows = slice(h * DK, (h + 1) * DK)
        keys = slice(h * DK, (h + 1) * DK)
        cols = slice(h * DV, (h + 1) * DV)
        s_in = ret_ref[rows, 0:DV].astype(f32)
        braw = braw_ref[:, cols]
        vd = jnp.where(tri(True), dot(braw, v, 1, 1, True), 0.0)
        dq = up * dot(vd, ki, 1, 0, True) + jnp.exp(r) * dot(braw, s_in, 1, 1, True)
        dk = down * dot(vd, qd, 0, 0, True)
        dv = dot(scores, braw, 0, 0, True)
        qo_ref[:, keys] = (dq * SCALE).astype(bf16)
        dk_ref[:, keys] = dk
        dv_ref[:, cols] = dv
        dd_ref[:, keys] = q * dq - k * dk


def final_kernel(
    k_ref, v_ref, a_ref, ret_ref, fut_ref, dk_ref, dv_ref, dd_ref, ko_ref, vo_ref, do_ref
):
    lower = tri(True).astype(f32)
    upper = tri(False).astype(f32)
    ones = jnp.ones((TOK, 128), f32)
    ones_row = jnp.ones((8, DV), f32)
    for h in range(HEADS):
        rows = slice(h * DK, (h + 1) * DK)
        keys = slice(h * DK, (h + 1) * DK)
        cols = slice(h * DV, (h + 1) * DV)
        a = head_cols(a_ref, h, DK)
        k = head_cols(k_ref, h, DK)
        v = head_cols(v_ref, h, DV)
        r = dot(lower, a, 1, 0, True)
        to_end = jnp.exp(r[TOK - 1 :, :] - r)
        ke = k * to_end
        fut = fut_ref[rows, :].astype(f32)
        s_in = ret_ref[rows, 0:DV].astype(f32)
        decay = jnp.exp(dot(a, ones, 0, 0, True))[:, 0:1]
        s_end = decay * s_in + dot(ke, v, 0, 0, True)
        cross = dot(ones_row, s_end * fut, 1, 1, True)[0:1, :]
        more = to_end * dot(v, fut, 1, 1, True)
        ko_ref[:, keys] = (dk_ref[:, keys] + more).astype(bf16)
        vo_ref[:, cols] = (dv_ref[:, cols] + dot(ke, fut, 1, 0, True)).astype(bf16)
        back = dd_ref[:, keys] - k * more
        do_ref[:, keys] = dot(upper, back, 1, 0, True) + cross


def outer_kernel(og_ref, out_ref):
    total = dot(og_ref[0, :, 0:HID], og_ref[0, :, HID:], 0, 0)
    for z in range(1, 4):
        total = total + dot(og_ref[z, :, 0:HID], og_ref[z, :, HID:], 0, 0)
    out_ref[...] = total.astype(bf16)


def shape(dims, dtype):
    return jax.ShapeDtypeStruct(dims, dtype)


def swapped(x):
    return lax.ppermute(x, "tp", [(0, 1), (1, 0)])


def exchanged(x, axes, count):
    parts = x.reshape(count, x.shape[0] // count, *x.shape[1:])
    return lax.all_to_all(parts, axes, split_axis=0, concat_axis=0, tiled=True).reshape(x.shape)


def body(
    mid_rows,
    cotangent,
    route_experts,
    route_weights,
    gate_weight,
    up_weight,
    down_weight,
    out_weight,
    queries,
    key_rows,
    value_rows,
    log_decay,
):
    core = lax.axis_index("tp").astype(jnp.int32).reshape(1)
    route = jnp.concatenate([route_experts.astype(f32), route_weights], axis=1)
    mid2, cot2, route2 = swapped(mid_rows), swapped(cotangent), swapped(route)
    gate, up, down = gate_weight[0], up_weight[0], down_weight[0]
    state_msg = call(
        state_kernel, shape((HEADS * DK, SW), bf16), (key_rows, value_rows, log_decay), name="state", flops=1 << 28
    )
    send, pick = call(
        pack_kernel,
        (shape((8 * NDEV, MSG), bf16), shape((8 * NDEV, 2 * ROWS), bf16)),
        (core, route, route2, mid_rows, mid2, cotangent, cot2, state_msg),
        [SMEM] + [None] * 7,
        name="pack",
        flops=1 << 28,
    )
    got = exchanged(send, SP, NDEV)
    theirs = swapped(got)
    scan_scratch = [pltpu.VMEM((8 * NDEV, DV), f32)] * 3
    state_spec = pl.BlockSpec((8 * NDEV, DV), lambda i: (0, 0))
    decay_spec = pl.BlockSpec((8 * NDEV, 128), lambda i: (0, DV // 128))

    def scanned(msg, decays, reverse):
        return pl.pallas_call(
            functools.partial(scan_kernel, reverse=reverse),
            grid=(1,),
            out_shape=shape((8 * NDEV, DV), bf16),
            in_specs=[state_spec, decay_spec],
            out_specs=state_spec,
            scratch_shapes=scan_scratch,
            name="scan",
        )(msg, decays)

    state_in = scanned(got, got, False)
    keep, give, rows_in, scaled, hidden, back_gate, back_up = call(
        expert_kernel,
        (shape((512, HALF), bf16), shape((512, HALF), bf16), shape((512, D), bf16), shape((512, D), bf16))
        + (shape((512, HID), bf16),) * 3,
        (core, got, theirs, gate, up, down),
        [SMEM, ANY, ANY, None, None, None],
        [pltpu.SemaphoreType.DMA((2,))],
        name="expert",
        flops=6 << 30,
    )
    summed = call(
        return_kernel, shape((512, RET), bf16), (keep, swapped(give), state_in), name="returned", flops=1 << 20
    )
    ret = exchanged(summed, SP, NDEV)
    gate_total = dot(rows_in, back_gate, 0, 0).astype(bf16)[None]
    up_total = dot(rows_in, back_up, 0, 0).astype(bf16)[None]
    down_total = dot(hidden, scaled, 0, 0).astype(bf16)[None]
    token_mine = call(
        combine_kernel,
        shape((TOK, HALF), bf16),
        (core, pick, ret, cotangent, cot2),
        [SMEM] + [None] * 4,
        name="combine",
        flops=1 << 26,
    )
    token_theirs = swapped(token_mine)
    back_msg, og, braw = call(
        mixer_kernel,
        (shape((512, DV), bf16), shape((4, TOK, HID + HALF), bf16), shape((TOK, HALF), f32)),
        (core, token_mine, token_theirs, out_weight, queries, key_rows, value_rows, log_decay, ret),
        [SMEM] + [None] * 8,
        name="mixer",
        flops=1 << 30,
    )
    back_got = exchanged(back_msg, SP, NDEV)
    og_got = lax.all_to_all(og, "sp_0", split_axis=0, concat_axis=0, tiled=True)
    query_out, dk_part, dv_part, dd_part = call(
        local_kernel,
        (shape((TOK, 512), bf16), shape((TOK, 512), f32), shape((TOK, HALF), f32), shape((TOK, 512), f32)),
        (queries, key_rows, value_rows, log_decay, ret, braw),
        name="local",
        flops=1 << 30,
    )
    future = exchanged(scanned(back_got, got, True), SP, NDEV)
    outer = call(outer_kernel, shape((512, HALF), bf16), (og_got,), name="outer", flops=1 << 29)
    terms = lax.all_to_all(
        outer.reshape(16, 32, HALF), ("sp_1", "sp_2"), split_axis=0, concat_axis=0, tiled=True
    )
    out_total = terms.astype(f32).sum(axis=0)
    key_out, value_out, decay_out = call(
        final_kernel,
        (shape((TOK, 512), bf16), shape((TOK, HALF), bf16), shape((TOK, 512), f32)),
        (key_rows, value_rows, log_decay, ret, future, dk_part, dv_part, dd_part),
        name="final",
        flops=1 << 29,
    )
    return (gate_total, up_total, down_total, out_total, query_out, key_out, value_out, decay_out)


def solution(mesh):
    split = Mesh(mesh.devices.reshape(4, 4, 4, mesh.shape["tp"]), ("sp_0", "sp_1", "sp_2", "tp"))
    placed = (
        P(SP_TP, None),
        P(SP_TP, None),
        P(SP_TP, None),
        P(SP_TP, None),
        P(SP, None, "tp"),
        P(SP, None, "tp"),
        P(SP, "tp", None),
        P(None, "tp"),
        P(SP, "tp"),
        P(SP, "tp"),
        P(SP, "tp"),
        P(SP, "tp"),
    )
    return jax.shard_map(
        body,
        mesh=split,
        in_specs=placed,
        out_specs=(
            P(SP, None, "tp"),
            P(SP, None, "tp"),
            P(SP, "tp", None),
            P(SP, "tp"),
            P(SP, "tp"),
            P(SP, "tp"),
            P(SP, "tp"),
            P(SP, "tp"),
        ),
        check_vma=False,
    )
```

profile of v0, /device:TPU:0, one launch (start us, length us, event | category | flops | bytes accessed | tf_op | source)
XLA Modules:
  0.0 209.2 jit_solution(10679767563961599861)
XLA Ops:
  2.9 3.1 %state.1.st_ref = bf16[512,384]{1,0:T(8,128)(2,1)} custom-call(bf16[128,512]{1,0:T(8,128)(2,1)} %k_ref.7, bf16[128,1024]{1,0:T(8,128)(2,1)} %v_ref.7, f32[128,512]{1,0:T(8,128)} %a_ref.7), custom_call_target="tpu_custom_call" | custom-call | flops 268435456 | bytes 1048576 | tf_op jit(solution)/shard_map/state/pallas_call | solution.py:46
  6.8 6.3 %pack.1 = (bf16[512,2432]{1,0:T(8,128)(2,1)}, bf16[512,128]{1,0:T(8,128)(2,1)}) custom-call(s32[1]{0:T(128)} %bitcast.core_ref, f32[64,4]{1,0:T(8,128)} %copy-done.7, f32[64,4]{1,0:T(8,128)} %copy-done.8, bf16[64,2048]{1,0:T(8,128)(2,1)} %mid_ref.1, bf16[64,2048]{1,0:T(8,128)(2,1)} %copy-done.6, bf16[64,2048]{1,0:T(8,128)(2,1)} %cot_ref.3, ...), custom_call_target="tpu_custom_call" | custom-call | flops 268435456 | bytes 1048576 | tf_op jit(solution)/shard_map/pack/pallas_call | solution.py:46
  13.1 46.6 %all_to_all.30 = bf16[64,8,2432]{2,1,0:T(8,128)(2,1)S(1)} all-to-all(bf16[64,8,2432]{2,1,0:T(8,128)(2,1)} %bitcast.36), channel_id=1, replica_groups=mesh['sp_0'=4,'sp_1'=4,'sp_2'=4,'tp'=2] {'sp_0','sp_1','sp_2'}, dimensions={0} | all-to-all | bytes 4980736 | tf_op jit(solution)/shard_map/all_to_all | solution.py:325
  59.7 4.7 %collective-permute-done.3.theirs_ref = bf16[512,2432]{1,0:T(8,128)(2,1)S(1)} collective-permute-done((bf16[512,2432]{1,0:T(8,128)(2,1)S(1)}, bf16[512,2432]{1,0:T(8,128)(2,1)S(1)}, u32[]{:S(2)}, u32[]{:S(2)}) %collective-permute-start.3) | collective-permute-done | bytes 2490400 | tf_op jit(solution)/shard_map/ppermute | solution.py:320
  65.9 11.8 %expert.1 = (bf16[512,1024]{1,0:T(8,128)(2,1)}, bf16[512,1024]{1,0:T(8,128)(2,1)}, bf16[512,2048]{1,0:T(8,128)(2,1)}, bf16[512,2048]{1,0:T(8,128)(2,1)}, bf16[51...) custom-call(s32[1]{0:T(128)} %bitcast.core_ref, bf16[512,2432]{1,0:T(8,128)(2,1)} %bitcast.26, ...), custom_call_target="tpu_custom_call" | custom-call | flops 6442450944 | bytes 1048576 | tf_op jit(solution)/shard_map/expert/pallas_call | solution.py:46
  77.9 1.9 scan.2.state_ref
  81.6 2.9 %returned.1 = bf16[512,1280]{1,0:T(8,128)(2,1)} custom-call(bf16[512,1024]{1,0:T(8,128)(2,1)} %get-tuple-element.34.keep_ref, bf16[512,1024]{1,0:T(8,128)(2,1)} %copy-done.2, bf16[512,256]{1,0:T(8,128)(2,1)} %scan.2.state_ref), custom_call_target="tpu_custom_call" | custom-call | flops 1048576 | bytes 1048576 | tf_op jit(solution)/shard_map/returned/pallas_call | solution.py:46
  84.5 27.8 %all_to_all.31 = bf16[64,8,1280]{2,1,0:T(8,128)(2,1)} all-to-all(bf16[64,8,1280]{2,1,0:T(8,128)(2,1)} %bitcast.34), channel_id=1, replica_groups=mesh['sp_0'=4,'sp_1'=4,'sp_2'=4,'tp'=2] {'sp_0','sp_1','sp_2'}, dimensions={0} | all-to-all | bytes 2621440 | tf_op jit(solution)/shard_map/all_to_all | solution.py:325
  112.3 2.7 %combine.1.mine_ref = bf16[128,1024]{1,0:T(8,128)(2,1)} custom-call(s32[1]{0:T(128)} %bitcast.core_ref, bf16[512,128]{1,0:T(8,128)(2,1)} %get-tuple-element.33.pick_ref, bf16[512,1280]{1,0:T(8,128)(2,1)} %bitcast.30, bf16[64,2048]{1,0:T(8,128)(2,1)} %cot_ref.3, bf16[64,2048]{1,0:T(8,128)(2,1)} %copy-done.4), custom_call_target="tpu_custom_call" | custom-call | flops 67108864 | bytes 1048576 | tf_op jit(solution)/shard_map/combine/pallas_call | solution.py:46
  115.0 1.7 collective-permute-done.5.theirs_ref
  117.4 9.8 %mixer.1 = (bf16[512,256]{1,0:T(8,128)(2,1)}, bf16[4,128,1536]{2,1,0:T(8,128)(2,1)}, f32[128,1024]{1,0:T(8,128)}) custom-call(s32[1]{0:T(128)} %bitcast.core_ref, bf16[128,1024]{1,0:T(8,128)(2,1)} %combine.1.mine_ref, bf16[128,1024]{1,0:T(8,128)(2,1)} %copy-done.5, bf16[2048,1024]{1,0:T(8,128)(2,1)} %w_ref.1, bf16[128,512]{1,0:T(8,128)(2,1)} %q_ref.3, ...), custom_call_target="tpu_custom_call" | custom-call | flops 1073741824 | bytes 1048576 | tf_op jit(solution)/shard_map/mixer/pallas_call | solution.py:46
  127.2 16.6 %all_to_all.32 = bf16[64,8,256]{2,1,0:T(8,128)(2,1)} all-to-all(bf16[64,8,256]{2,1,0:T(8,128)(2,1)} %bitcast.40), channel_id=1, replica_groups=mesh['sp_0'=4,'sp_1'=4,'sp_2'=4,'tp'=2] {'sp_0','sp_1','sp_2'}, dimensions={0} | all-to-all | bytes 524288 | tf_op jit(solution)/shard_map/all_to_all | solution.py:325
  143.8 3.6 %all-to-all-start.2 = ((bf16[4,128,1536]{2,1,0:T(8,128)(2,1)}), bf16[4,128,1536]{2,1,0:T(8,128)(2,1)S(1)}, u32[]{:S(2)}, u32[]{:S(2)}) async-start(bf16[4,128,1536]{2,1,0:T(8,128)(2,1)} %get-tuple-element.36), calls=%async_computation.2 | async-start | bytes 3145728 | tf_op jit(solution)/shard_map/all_to_all | solution.py:410
  147.3 1.9 scan.3
  149.2 18.3 %all-to-all-done.2.og_ref = bf16[4,128,1536]{2,1,0:T(8,128)(2,1)S(1)} async-done(((bf16[4,128,1536]{2,1,0:T(8,128)(2,1)}), bf16[4,128,1536]{2,1,0:T(8,128)(2,1)S(1)}, u32[]{:S(2)}, u32[]{:S(2)}) %all-to-all-start.2) | async-done | bytes 1572896 | tf_op jit(solution)/shard_map/all_to_all | solution.py:410
  167.5 4.7 %all-to-all-start.5 = ((bf16[64,8,256]{2,1,0:T(8,128)(2,1)}), bf16[64,8,256]{2,1,0:T(8,128)(2,1)S(1)}, u32[]{:S(2)}, u32[]{:S(2)}) async-start(bf16[64,8,256]{2,1,0:T(8,128)(2,1)} %bitcast.38), calls=%async_computation.5 | async-start | bytes 524288 | tf_op jit(solution)/shard_map/all_to_all | solution.py:325
  172.2 3.7 %outer.1 = bf16[512,1024]{1,0:T(8,128)(2,1)} custom-call(bf16[4,128,1536]{2,1,0:T(8,128)(2,1)} %copy-done.1), custom_call_target="tpu_custom_call" | custom-call | flops 536870912 | bytes 1048576 | tf_op jit(solution)/shard_map/outer/pallas_call | solution.py:46
  175.9 6.9 %all-to-all-done.5 = bf16[64,8,256]{2,1,0:T(8,128)(2,1)S(1)} async-done(((bf16[64,8,256]{2,1,0:T(8,128)(2,1)}), bf16[64,8,256]{2,1,0:T(8,128)(2,1)S(1)}, u32[]{:S(2)}, u32[]{:S(2)}) %all-to-all-start.5) | async-done | bytes 262176 | tf_op jit(solution)/shard_map/all_to_all | solution.py:325
  182.8 3.9 %all-to-all-start.3 = ((bf16[16,32,1024]{2,1,0:T(8,128)(2,1)}), bf16[16,32,1024]{2,1,0:T(8,128)(2,1)S(1)}, u32[]{:S(2)}, u32[]{:S(2)}) async-start(bf16[16,32,1024]{2,1,0:T(8,128)(2,1)} %bitcast.35), calls=%async_computation.3 | async-start | bytes 2097152 | tf_op jit(solution)/shard_map/all_to_all | solution.py:420
  186.7 3.7 %fusion.1 = bf16[1,2048,512]{2,1,0:T(8,128)(2,1)} fusion(bf16[512,2048]{1,0:T(8,128)(2,1)S(1)} %copy-done.12, bf16[512,512]{1,0:T(8,128)(2,1)} %get-tuple-element.30), kind=kOutput, calls=%fused_computation.4 | convolution fusion | flops 1074790400 | bytes 4718592 | tf_op jit(solution)/shard_map/dot_general | solution.py:33
  190.5 2.6 %fusion = bf16[1,2048,512]{2,1,0:T(8,128)(2,1)} fusion(bf16[512,2048]{1,0:T(8,128)(2,1)S(1)} %copy-done.12, bf16[512,512]{1,0:T(8,128)(2,1)S(1)} %copy-done.13), kind=kOutput, calls=%fused_computation.3 | convolution fusion | flops 1074790400 | bytes 4718592 | tf_op jit(solution)/shard_map/dot_general | solution.py:33
  193.1 2.6 %fusion.2 = bf16[1,512,2048]{2,1,0:T(8,128)(2,1)} fusion(bf16[512,512]{1,0:T(8,128)(2,1)S(1)} %copy-done.11, bf16[512,2048]{1,0:T(8,128)(2,1)S(1)} %copy-done.10), kind=kOutput, calls=%fused_computation.5 | convolution fusion | flops 1074790400 | bytes 4718592 | tf_op jit(solution)/shard_map/dot_general | solution.py:33
  195.7 5.9 %local.1 = (bf16[128,512]{1,0:T(8,128)(2,1)}, f32[128,512]{1,0:T(8,128)}, f32[128,1024]{1,0:T(8,128)}, f32[128,512]{1,0:T(8,128)}) custom-call(bf16[128,512]{1,0:T(8,128)(2,1)} %q_ref.3, bf16[128,512]{1,0:T(8,128)(2,1)} %k_ref.7, bf16[128,1024]{1,0:T(8,128)(2,1)} %v_ref.7, f32[128,512]{1,0:T(8,128)} %a_ref.7, bf16[512,1280]{1,0:T(8,128)(2,1)} %bitcast.32, ...), custom_call_target="tpu_custom_call" | custom-call | flops 1073741824 | bytes 1048576 | tf_op jit(solution)/shard_map/local/pallas_call | solution.py:46
  201.5 6.9 %final.1 = (bf16[128,512]{1,0:T(8,128)(2,1)}, bf16[128,1024]{1,0:T(8,128)(2,1)}, f32[128,512]{1,0:T(8,128)}) custom-call(bf16[128,512]{1,0:T(8,128)(2,1)} %k_ref.7, bf16[128,1024]{1,0:T(8,128)(2,1)} %v_ref.7, f32[128,512]{1,0:T(8,128)} %a_ref.7, bf16[512,1280]{1,0:T(8,128)(2,1)} %bitcast.33, bf16[512,256]{1,0:T(8,128)(2,1)} %bitcast.37, ...), custom_call_target="tpu_custom_call" | custom-call | flops 536870912 | bytes 1048576 | tf_op jit(solution)/shard_map/final/pallas_call | solution.py:46
  (43 shorter events, 8.1 us)
Async XLA Ops:
  0.6 5.3 %collective-permute-start.2 = (bf16[64,2048]{1,0:T(8,128)(2,1)}, bf16[64,2048]{1,0:T(8,128)(2,1)S(1)}, u32[]{:S(2)}, u32[]{:S(2)}) collective-permute-start(bf16[64,2048]{1,0:T(8,128)(2,1)} %cot_ref.3), channel_id=1, source_target_pairs={{0,1},{1,0},{2,3},{3,2},{4,5},{5,4},{6,7},{7,6},{8,9},{9,8},{10,11... | collective-permute-start | bytes 786440 | tf_op jit(solution)/shard_map/ppermute | solution.py:320
  0.7 5.3 %collective-permute-start.1 = (bf16[64,2048]{1,0:T(8,128)(2,1)}, bf16[64,2048]{1,0:T(8,128)(2,1)S(1)}, u32[]{:S(2)}, u32[]{:S(2)}) collective-permute-start(bf16[64,2048]{1,0:T(8,128)(2,1)} %mid_ref.1), channel_id=1, source_target_pairs={{0,1},{1,0},{2,3},{3,2},{4,5},{5,4},{6,7},{7,6},{8,9},{9,8},{10,11... | collective-permute-start | bytes 786440 | tf_op jit(solution)/shard_map/ppermute | solution.py:320
  2.7 3.3 %copy-start.7 = (f32[64,4]{1,0:T(8,128)}, f32[64,4]{1,0:T(8,128)S(1)}, u32[]{:S(2)}) copy-start(f32[64,4]{1,0:T(8,128)S(1)} %copy.23.route_ref) | copy-start | bytes 3076
  2.7 3.3 %collective-permute-start = (f32[64,4]{1,0:T(8,128)S(1)}, f32[64,4]{1,0:T(8,128)S(1)}, u32[]{:S(2)}, u32[]{:S(2)}) collective-permute-start(f32[64,4]{1,0:T(8,128)S(1)} %copy.23.route_ref), channel_id=1, source_target_pairs={{0,1},{1,0},{2,3},{3,2},{4,5},{5,4},{6,7},{7,6},{8,9},{9,8},{10,11... | collective-permute-start | bytes 3080 | tf_op jit(solution)/shard_map/ppermute | solution.py:320
  6.0 0.6 copy-start.8
  6.0 0.7 copy-start.4
  6.0 0.8 copy-start.6
  59.7 4.7 %copy-start = (bf16[64,8,2432]{2,1,0:T(8,128)(2,1)}, bf16[64,8,2432]{2,1,0:T(8,128)(2,1)S(1)}, u32[]{:S(2)}) copy-start(bf16[64,8,2432]{2,1,0:T(8,128)(2,1)S(1)} %all_to_all.30) | copy-start | bytes 7471108
  59.7 4.7 %collective-permute-start.3 = (bf16[512,2432]{1,0:T(8,128)(2,1)S(1)}, bf16[512,2432]{1,0:T(8,128)(2,1)S(1)}, u32[]{:S(2)}, u32[]{:S(2)}) collective-permute-start(bf16[512,2432]{1,0:T(8,128)(2,1)S(1)} %bitcast.25), channel_id=1, source_target_pairs={{0,1},{1,0},{2,3},{3,2},{4,5},{5,4},{6,7},{7,6},{8,9},{9,8},{10,11... | collective-permute-start | bytes 7471112 | tf_op jit(solution)/shard_map/ppermute | solution.py:320
  64.4 1.5 copy-start.9
  77.6 3.0 %collective-permute-start.4 = (bf16[512,1024]{1,0:T(8,128)(2,1)}, bf16[512,1024]{1,0:T(8,128)(2,1)S(1)}, u32[]{:S(2)}, u32[]{:S(2)}) collective-permute-start(bf16[512,1024]{1,0:T(8,128)(2,1)} %get-tuple-element.35), channel_id=1, source_target_pairs={{0,1},{1,0},{2,3},{3,2},{4,5},{5,4},{6,7},{7,6},{8,9},{9,8},{10,11... | collective-permute-start | bytes 3145736 | tf_op jit(solution)/shard_map/ppermute | solution.py:320
  80.6 1.0 copy-start.2
  115.0 1.7 collective-permute-start.5
  116.7 0.7 copy-start.5
  143.8 23.8 %all-to-all-start.2 = ((bf16[4,128,1536]{2,1,0:T(8,128)(2,1)}), bf16[4,128,1536]{2,1,0:T(8,128)(2,1)S(1)}, u32[]{:S(2)}, u32[]{:S(2)}) async-start(bf16[4,128,1536]{2,1,0:T(8,128)(2,1)} %get-tuple-element.36), calls=%async_computation.2 | async-start | bytes 3145728 | tf_op jit(solution)/shard_map/all_to_all | solution.py:410
  167.5 4.7 %copy-start.1 = (bf16[4,128,1536]{2,1,0:T(8,128)(2,1)}, bf16[4,128,1536]{2,1,0:T(8,128)(2,1)S(1)}, u32[]{:S(2)}) copy-start(bf16[4,128,1536]{2,1,0:T(8,128)(2,1)S(1)} %all-to-all-done.2.og_ref) | copy-start | bytes 4718596
  167.5 15.3 %all-to-all-start.5 = ((bf16[64,8,256]{2,1,0:T(8,128)(2,1)}), bf16[64,8,256]{2,1,0:T(8,128)(2,1)S(1)}, u32[]{:S(2)}, u32[]{:S(2)}) async-start(bf16[64,8,256]{2,1,0:T(8,128)(2,1)} %bitcast.38), calls=%async_computation.5 | async-start | bytes 524288 | tf_op jit(solution)/shard_map/all_to_all | solution.py:325
  175.9 10.8 %copy-start.12 = (bf16[512,2048]{1,0:T(8,128)(2,1)S(1)}, bf16[512,2048]{1,0:T(8,128)(2,1)}, u32[]{:S(2)}) copy-start(bf16[512,2048]{1,0:T(8,128)(2,1)} %get-tuple-element.28) | copy-start | bytes 6291460
  182.8 7.6 %copy-start.3 = (bf16[64,8,256]{2,1,0:T(8,128)(2,1)}, bf16[64,8,256]{2,1,0:T(8,128)(2,1)S(1)}, u32[]{:S(2)}) copy-start(bf16[64,8,256]{2,1,0:T(8,128)(2,1)S(1)} %all-to-all-done.5) | copy-start | bytes 786436
  182.8 25.6 %all-to-all-start.3 = ((bf16[16,32,1024]{2,1,0:T(8,128)(2,1)}), bf16[16,32,1024]{2,1,0:T(8,128)(2,1)S(1)}, u32[]{:S(2)}, u32[]{:S(2)}) async-start(bf16[16,32,1024]{2,1,0:T(8,128)(2,1)} %bitcast.35), calls=%async_computation.3 | async-start | bytes 2097152 | tf_op jit(solution)/shard_map/all_to_all | solution.py:420
  186.7 3.7 %copy-start.13 = (bf16[512,512]{1,0:T(8,128)(2,1)S(1)}, bf16[512,512]{1,0:T(8,128)(2,1)}, u32[]{:S(2)}) copy-start(bf16[512,512]{1,0:T(8,128)(2,1)} %get-tuple-element.29) | copy-start | bytes 1572868
  190.4 2.6 %copy-start.10 = (bf16[512,2048]{1,0:T(8,128)(2,1)S(1)}, bf16[512,2048]{1,0:T(8,128)(2,1)}, u32[]{:S(2)}) copy-start(bf16[512,2048]{1,0:T(8,128)(2,1)} %get-tuple-element.32) | copy-start | bytes 6291460
  190.4 2.6 %copy-start.11 = (bf16[512,512]{1,0:T(8,128)(2,1)S(1)}, bf16[512,512]{1,0:T(8,128)(2,1)}, u32[]{:S(2)}) copy-start(bf16[512,512]{1,0:T(8,128)(2,1)} %get-tuple-element.31) | copy-start | bytes 1572868
where the time goes:
time: 210 us; the launch traced here: 209 us
  blocking collectives  90.9 us (43%)
  Pallas kernels  56.7 us (27%)
  waiting for transfers between devices  32.5 us (15%)
  starting transfers between devices  13.1 us (6%)
  matrix products  8.93 us (4%)
  local copies, waits for them, and re-layouts  4.04 us (2%)
  other arithmetic  2.21 us (1%)
    all_to_all x3, blocking collectives, exchanged(): lax.all_to_all(parts, axes, split_axis=0, concat_axis=0, tiled=True)  90.9 us
    pallas_call x9, Pallas kernels, call(): pl.pallas_call(kernel, out_shape=out_shape, in_specs=[s or vmem for s in...  52.9 us
    all_to_all x1, waiting for transfers between devices, body(): og_got = lax.all_to_all(og, 'sp_0', split_axis=0, concat_axis=0, tiled=True)  18.3 us
    dot_general x3, matrix products, dot(): lax.dot_general(a, b, (((ca,), (cb,)), ((), ())), precision=lax.Precision...  8.93 us
    ppermute x6, waiting for transfers between devices, swapped(): return lax.ppermute(x, 'tp', [(0, 1), (1, 0)])  7.3 us
    all_to_all x1, waiting for transfers between devices, exchanged(): lax.all_to_all(parts, axes, split_axis=0, concat_axis=0, tiled=True)  6.94 us
    all_to_all x1, starting transfers between devices, exchanged(): lax.all_to_all(parts, axes, split_axis=0, concat_axis=0, tiled=True)  4.68 us
  transfers between devices with their start and end apart: 9, of which 5 were waited for; matrix products, arithmetic and copies ran while one was open for 5% of the time, Pallas kernels for 11%

commit v1 on v0

v1 whole, which is shorter than its diff:
```python
import functools

import jax
import jax.numpy as jnp
from jax import lax
from jax.experimental import pallas as pl
from jax.experimental.pallas import tpu as pltpu
from jax.sharding import Mesh
from jax.sharding import PartitionSpec as P


DK = 128
DV = 256
SP = ("sp_0", "sp_1", "sp_2")
SP_TP = ("sp_0", "sp_1", "sp_2", "tp")
ROWS = 64
D = 2048
HALF = 1024
HID = 512
HEADS = 4
TOK = 128
NDEV = 64
SW = DV + 128
MSG = SW + D
SCALE = DK**-0.5


f32 = jnp.float32
bf16 = jnp.bfloat16
epsilon = 1e-06


def dot(a, b, ca, cb, high=False):
    return lax.dot_general(
        a,
        b,
        (((ca,), (cb,)), ((), ())),
        precision=lax.Precision.HIGHEST if high else None,
        preferred_element_type=f32,
    )


def fast(dims, dtype):
    return pltpu.VMEM(dims, dtype)


def far_out(dims, dtype):
    return pltpu.HBM(dims, dtype)


SMEM, NEAR, FAR = "s", "n", "f"


def call(kernel, out_shape, args, kinds, scratch=(), flops=0, limit=12, manual=()):
    vmem = pl.BlockSpec(memory_space=pltpu.VMEM)
    specs = {SMEM: pl.BlockSpec(memory_space=pltpu.SMEM), FAR: pl.BlockSpec(memory_space=pl.ANY)}
    spaces = {NEAR: pltpu.VMEM, FAR: pltpu.HBM}
    many = isinstance(out_shape, (list, tuple))
    outs = list(out_shape) if many else [out_shape]
    out_specs = [specs[FAR] if i in manual else vmem for i in range(len(outs))]
    args = [
        pltpu.with_memory_space_constraint(a, spaces[k]) if k in spaces else a for a, k in zip(args, kinds)
    ]
    return pl.pallas_call(
        kernel,
        out_shape=out_shape,
        in_specs=[specs.get(k, vmem) for k in kinds],
        out_specs=out_specs if many else out_specs[0],
        scratch_shapes=list(scratch),
        compiler_params=pltpu.CompilerParams(vmem_limit_bytes=limit * 1024 * 1024),
        cost_estimate=pl.CostEstimate(flops=flops, transcendentals=0, bytes_accessed=1 << 20),
    )(*args)


def tri(lower):
    i = lax.broadcasted_iota(jnp.int32, (TOK, TOK), 0)
    j = lax.broadcasted_iota(jnp.int32, (TOK, TOK), 1)
    return (i >= j) if lower else (i <= j)


def head_cols(ref, h, width):
    return ref[:, h * width : (h + 1) * width].astype(f32)


def state_kernel(k_ref, v_ref, a_ref, msg_ref):
    lower = tri(True).astype(f32)
    ones = jnp.ones((TOK, 128), f32)
    lane = lax.broadcasted_iota(jnp.int32, (DK, 128), 1)
    for h in range(HEADS):
        a = head_cols(a_ref, h, DK)
        r = dot(lower, a, 1, 0, True)
        ke = head_cols(k_ref, h, DK) * jnp.exp(r[TOK - 1 :, :] - r)
        s = dot(ke, head_cols(v_ref, h, DV), 0, 0, True)
        rows = slice(h * DK, (h + 1) * DK)
        msg_ref[rows, 0:DV] = s.astype(bf16)
        col = dot(a, ones, 0, 0, True)
        hi = col.astype(bf16).astype(f32)
        mid = (col - hi).astype(bf16).astype(f32)
        lo = col - hi - mid
        part = jnp.where(lane == 0, hi, jnp.where(lane == 1, mid, jnp.where(lane == 2, lo, 0.0)))
        msg_ref[rows, DV:SW] = part.astype(bf16)


def pack_kernel(
    core_ref, ids_ref, ids2_ref, wts_ref, wts2_ref, mid_ref, mid2_ref, cot_ref, cot2_ref, state_ref,
    out_ref, pick_ref, rows_ref, send_ref, pick_v_ref, sems,
):
    core = core_ref[0]

    @pl.when(core == 0)
    def _():
        pltpu.make_async_copy(mid_ref, rows_ref.at[0:ROWS], sems.at[0]).start()
        pltpu.make_async_copy(mid2_ref, rows_ref.at[ROWS : 2 * ROWS], sems.at[1]).start()

    @pl.when(core == 1)
    def _():
        pltpu.make_async_copy(cot_ref, rows_ref.at[0:ROWS], sems.at[0]).start()
        pltpu.make_async_copy(cot2_ref, rows_ref.at[ROWS : 2 * ROWS], sems.at[1]).start()

    state_out = pltpu.make_async_copy(state_ref, out_ref.at[:, 0:SW], sems.at[7])
    state_out.start()
    expert = lax.broadcasted_iota(jnp.int32, (NDEV, ROWS), 0)
    ti = lax.broadcasted_iota(jnp.int32, (ROWS, ROWS), 0)
    tj = lax.broadcasted_iota(jnp.int32, (ROWS, ROWS), 1)
    before = (ti < tj).astype(bf16)
    si = lax.broadcasted_iota(jnp.int32, (8 * NDEV, NDEV), 0)
    se = lax.broadcasted_iota(jnp.int32, (8 * NDEV, NDEV), 1)
    expand = (si // 8 == se).astype(bf16)
    slot = (si % 4 + 1).astype(f32)
    owner = (si % 8) // 4

    def picks(ids, wts, which):
        e1 = (ids[0:1, :] == expert).astype(f32)
        e2 = (ids[1:2, :] == expert).astype(f32)
        both = e1 + e2
        rank = both * (dot(both.astype(bf16), before, 1, 0) + 1.0)
        weight = e1 * wts[0:1, :] + e2 * wts[1:2, :]
        found = dot(expand, rank.astype(bf16), 1, 0)
        return jnp.where((found == slot) & (owner == which), 1.0, 0.0), weight

    own, weight_own = picks(ids_ref, wts_ref, core)
    other, weight_other = picks(ids2_ref, wts2_ref, 1 - core)
    pick_v_ref[:, 0:ROWS] = own.astype(bf16)
    pick_v_ref[:, ROWS:] = other.astype(bf16)
    pick_out = pltpu.make_async_copy(pick_v_ref, pick_ref, sems.at[2])
    pick_out.start()
    wide = expand.astype(f32)
    w = own * dot(wide, weight_own, 1, 0, True) + other * dot(wide, weight_other, 1, 0, True)
    scale = jnp.where(core == 0, 1.0, jnp.sum(w, axis=1, keepdims=True))
    pltpu.make_async_copy(mid_ref, rows_ref.at[0:ROWS], sems.at[0]).wait()
    pltpu.make_async_copy(mid2_ref, rows_ref.at[ROWS : 2 * ROWS], sems.at[1]).wait()
    outs = []
    for i in range(4):
        cols = slice(i * HID, (i + 1) * HID)
        rows = dot(pick_v_ref[...], rows_ref[:, cols], 1, 0)
        send_ref[:, cols] = (rows * scale).astype(bf16)
        to = out_ref.at[:, SW + i * HID : SW + (i + 1) * HID]
        outs.append(pltpu.make_async_copy(send_ref.at[:, cols], to, sems.at[3 + i]))
        outs[i].start()
    pick_out.wait()
    state_out.wait()
    for c in outs:
        c.wait()


def grads_kernel(
    core_ref, got_ref, other_ref, hidden_ref, bg_ref, bu_ref, gate_ref, up_ref, down_ref, rows_ref, scaled_ref, sems
):
    core = core_ref[0]
    got_ref = got_ref.at[:, SW:MSG]
    other_ref = other_ref.at[:, SW:MSG]

    @pl.when(core == 0)
    def _():
        pltpu.make_async_copy(got_ref, rows_ref, sems.at[0]).start()
        pltpu.make_async_copy(other_ref, scaled_ref, sems.at[1]).start()

    @pl.when(core == 1)
    def _():
        pltpu.make_async_copy(other_ref, rows_ref, sems.at[0]).start()
        pltpu.make_async_copy(got_ref, scaled_ref, sems.at[1]).start()

    pltpu.make_async_copy(got_ref, rows_ref, sems.at[0]).wait()
    pltpu.make_async_copy(got_ref, scaled_ref, sems.at[1]).wait()

    def part(i, carry):
        part = pl.ds(pl.multiple_of(i * HID, HID), HID)
        x = rows_ref[:, part]
        gate_ref[part, :] = dot(x, bg_ref[...], 0, 0).astype(bf16)
        up_ref[part, :] = dot(x, bu_ref[...], 0, 0).astype(bf16)
        down_ref[:, part] = dot(hidden_ref[...], scaled_ref[:, part], 0, 0).astype(bf16)
        return carry

    lax.fori_loop(0, 4, part, 0)


def load_kernel(*refs):
    count = (len(refs) - 1) // 2
    copies = [pltpu.make_async_copy(refs[i], refs[count + i], refs[-1].at[i]) for i in range(count)]
    for c in copies:
        c.start()
    for c in copies:
        c.wait()


def scan_kernel(*refs, reverse):
    got_ref, out_ref, part_ref, x_ref, d_ref, y_ref, sem = refs[-7:]
    copy = pltpu.make_async_copy(got_ref.at[:, 0:SW], part_ref, sem.at[0])
    copy.start()
    copy.wait()
    msg_ref = refs[0] if reverse else part_ref
    x_ref[...] = msg_ref[:, 0:DV].astype(f32)
    log = jnp.sum(part_ref[:, DV:].astype(f32), axis=1, keepdims=True)
    d_ref[...] = jnp.broadcast_to(jnp.exp(log), (8 * NDEV, DV))
    state = jnp.zeros((8, DV), f32)
    for n in range(NDEV):
        p = NDEV - 1 - n if reverse else n
        rows = slice(8 * p, 8 * p + 8)
        y_ref[rows, :] = state
        state = d_ref[rows, :] * state + x_ref[rows, :]
    out_ref[...] = y_ref[...].astype(bf16)


def expert_kernel(
    core_ref, mine_ref, theirs_ref, gate_ref, up_ref, down_ref,
    keep_ref, send_ref, hidden_out, bg_out, bu_out,
    rows_ref, scaled_ref, hidden_ref, bg_ref, bu_ref, sems,
):
    core = core_ref[0]
    mine_ref = mine_ref.at[:, SW:MSG]
    theirs_ref = theirs_ref.at[:, SW:MSG]

    @pl.when(core == 0)
    def _():
        pltpu.make_async_copy(mine_ref, rows_ref, sems.at[0]).start()
        pltpu.make_async_copy(theirs_ref, scaled_ref, sems.at[1]).start()

    @pl.when(core == 1)
    def _():
        pltpu.make_async_copy(theirs_ref, rows_ref, sems.at[0]).start()
        pltpu.make_async_copy(mine_ref, scaled_ref, sems.at[1]).start()

    pltpu.make_async_copy(mine_ref, rows_ref, sems.at[0]).wait()
    pre_gate = dot(rows_ref[...], gate_ref[...], 1, 0)
    pre_up = dot(rows_ref[...], up_ref[...], 1, 0)
    sig = 1.0 / (1.0 + jnp.exp(-pre_gate))
    swish = pre_gate * sig
    slope = sig * (1.0 + pre_gate * (1.0 - sig))
    hidden_ref[...] = (swish * pre_up).astype(bf16)
    hidden_copy = pltpu.make_async_copy(hidden_ref, hidden_out, sems.at[2])
    hidden_copy.start()
    pltpu.make_async_copy(mine_ref, scaled_ref, sems.at[1]).wait()
    back = dot(scaled_ref[...], down_ref[...], 1, 1)
    bg_ref[...] = (back * pre_up * slope).astype(bf16)
    bu_ref[...] = (back * swish).astype(bf16)
    bg_copy = pltpu.make_async_copy(bg_ref, bg_out, sems.at[3])
    bu_copy = pltpu.make_async_copy(bu_ref, bu_out, sems.at[4])
    bg_copy.start()
    bu_copy.start()

    def half(c):
        cols = pl.ds(pl.multiple_of(c * HALF, HALF), HALF)
        total = dot(bg_ref[...], gate_ref[cols, :], 1, 1) + dot(bu_ref[...], up_ref[cols, :], 1, 1)
        return total.astype(bf16)

    send_ref[...] = half(1 - core)
    keep_ref[...] = half(core)
    for c in (hidden_copy, bg_copy, bu_copy):
        c.wait()


def return_kernel(keep_ref, got_ref, out_ref):
    out_ref[...] = (keep_ref[...].astype(f32) + got_ref[...].astype(f32)).astype(bf16)


def combine_kernel(core_ref, pick_ref, ret_ref, cot_ref, cot2_ref, out_ref):
    core = core_ref[0]
    rows = ret_ref[...]
    cols = pl.ds(pl.multiple_of(core * HALF, HALF), HALF)

    def put(lanes, cot, which):
        total = dot(pick_ref[:, lanes], rows, 0, 0) + cot[:, cols].astype(f32)
        out_ref[pl.ds(pl.multiple_of(which * ROWS, ROWS), ROWS), :] = total.astype(bf16)

    put(slice(0, ROWS), cot_ref, core)
    put(slice(ROWS, 2 * ROWS), cot2_ref, 1 - core)


def forward_parts(q_ref, k_ref, v_ref, a_ref, h):
    lower = tri(True)
    r = dot(lower.astype(f32), head_cols(a_ref, h, DK), 1, 0, True)
    mid = r[TOK // 2 : TOK // 2 + 1, :]
    up = jnp.exp(r - mid)
    down = jnp.exp(mid - r)
    q = head_cols(q_ref, h, DK) * SCALE
    k = head_cols(k_ref, h, DK)
    v = head_cols(v_ref, h, DV)
    qd = q * up
    ki = k * down
    scores = jnp.where(lower, dot(qd, ki, 1, 1, True), 0.0)
    return r, up, down, q, k, v, qd, ki, scores


def prior_kernel(q_ref, k_ref, v_ref, a_ref, inner_ref, qabs_ref, ke_ref, toend_ref, sloc_ref):
    for h in range(HEADS):
        r, _, _, q, k, v, _, _, scores = forward_parts(q_ref, k_ref, v_ref, a_ref, h)
        keys = slice(h * DK, (h + 1) * DK)
        inner_ref[:, h * DV : (h + 1) * DV] = dot(scores, v, 1, 0, True)
        qabs_ref[:, keys] = q * jnp.exp(r)
        to_end = jnp.exp(r[TOK - 1 :, :] - r)
        ke = k * to_end
        ke_ref[:, keys] = ke
        toend_ref[:, keys] = to_end
        sloc_ref[keys, :] = dot(ke, v, 0, 0, True)


def forward_kernel(inner_ref, qabs_ref, sin_ref, sloc_ref, a_ref, normed_ref, inv_ref, rounded_ref, send_ref):
    ones = jnp.ones((TOK, 128), f32)
    for h in range(HEADS):
        keys = slice(h * DK, (h + 1) * DK)
        cols = slice(h * DV, (h + 1) * DV)
        s_in = sin_ref[keys, :].astype(f32)
        decay = jnp.exp(dot(a_ref[:, keys], ones, 0, 0, True))[:, 0:1]
        send_ref[keys, :] = decay * s_in + sloc_ref[keys, :]
        raw = inner_ref[:, cols] + dot(qabs_ref[:, keys], s_in, 1, 0, True)
        inv = lax.rsqrt(jnp.mean(raw * raw, axis=1, keepdims=True) + epsilon)
        normed = raw * inv
        normed_ref[:, cols] = normed
        inv_ref[:, keys] = jnp.broadcast_to(inv, (TOK, DK))
        rounded_ref[:, cols] = normed.astype(bf16)


def mixer_kernel(
    place_ref, mine_ref, theirs_ref, w_ref, qabs_ref, normed_ref, inv_ref,
    msg_ref, braw_ref, og0_ref, og1_ref, og2_ref, og3_ref,
):
    core = place_ref[0]
    z = place_ref[1]
    mine = mine_ref[...]
    theirs = theirs_ref[...]
    row_mine = pl.multiple_of(core * HALF, HALF)
    row_theirs = pl.multiple_of((1 - core) * HALF, HALF)
    for h in range(HEADS):
        keys = slice(h * DK, (h + 1) * DK)
        cols = slice(h * DV, (h + 1) * DV)
        bn = dot(mine, w_ref[pl.ds(row_mine, HALF), cols], 1, 0) + dot(
            theirs, w_ref[pl.ds(row_theirs, HALF), cols], 1, 0
        )
        normed = normed_ref[:, cols]
        inv = inv_ref[:, keys][:, 0:1]
        braw = inv * (bn - normed * jnp.mean(bn * normed, axis=1, keepdims=True))
        braw_ref[:, cols] = braw
        msg_ref[keys, :] = dot(qabs_ref[:, keys], braw, 0, 0, True).astype(bf16)
    for shift, ref in enumerate((og0_ref, og1_ref, og2_ref, og3_ref)):
        to = (z + shift) % 4
        cols = pl.ds(pl.multiple_of((to % 2) * HID, HID), HID)
        ref[...] = jnp.where(to // 2 == core, mine_ref[:, cols], theirs_ref[:, cols])


def local_kernel(
    q_ref, k_ref, v_ref, a_ref, sin_ref, braw_ref, qo_ref, dk_ref, dv_ref, dd_ref
):
    for h in range(HEADS):
        r, up, down, q, k, v, qd, ki, scores = forward_parts(q_ref, k_ref, v_ref, a_ref, h)
        rows = slice(h * DK, (h + 1) * DK)
        keys = slice(h * DK, (h + 1) * DK)
        cols = slice(h * DV, (h + 1) * DV)
        s_in = sin_ref[rows, :].astype(f32)
        braw = braw_ref[:, cols]
        vd = jnp.where(tri(True), dot(braw, v, 1, 1, True), 0.0)
        dq = up * dot(vd, ki, 1, 0, True) + jnp.exp(r) * dot(braw, s_in, 1, 1, True)
        dk = down * dot(vd, qd, 0, 0, True)
        dv = dot(scores, braw, 0, 0, True)
        qo_ref[:, keys] = (dq * SCALE).astype(bf16)
        dk_ref[:, keys] = dk
        dv_ref[:, cols] = dv
        dd_ref[:, keys] = q * dq - k * dk


def final_kernel(
    k_ref, v_ref, ke_ref, toend_ref, send_ref, fut_ref, dk_ref, dv_ref, dd_ref, ko_ref, vo_ref, do_ref
):
    upper = tri(False).astype(f32)
    ones_row = jnp.ones((8, DV), f32)
    for h in range(HEADS):
        rows = slice(h * DK, (h + 1) * DK)
        keys = slice(h * DK, (h + 1) * DK)
        cols = slice(h * DV, (h + 1) * DV)
        k = head_cols(k_ref, h, DK)
        fut = fut_ref[rows, :].astype(f32)
        cross = dot(ones_row, send_ref[rows, :] * fut, 1, 1, True)[0:1, :]
        more = toend_ref[:, keys] * dot(v_ref[:, cols], fut_ref[rows, :], 1, 1)
        ko_ref[:, keys] = (dk_ref[:, keys] + more).astype(bf16)
        vo_ref[:, cols] = (dv_ref[:, cols] + dot(ke_ref[:, keys], fut, 1, 0, True)).astype(bf16)
        back = dd_ref[:, keys] - k * more
        do_ref[:, keys] = dot(upper, back, 1, 0, True) + cross


def outer_kernel(*refs):
    total = dot(refs[0][...], refs[4][...], 0, 0)
    for n in range(1, 4):
        total = total + dot(refs[n][...], refs[4 + n][...], 0, 0)
    refs[8][...] = total.astype(bf16)


def total_kernel(terms_ref, out_ref):
    total = terms_ref[0].astype(f32)
    for n in range(1, 16):
        total = total + terms_ref[n].astype(f32)
    out_ref[...] = total


def swapped(x):
    return lax.ppermute(x, "tp", [(0, 1), (1, 0)])


def turned(x, axis, shift):
    return lax.ppermute(x, axis, [(n, (n + shift) % 4) for n in range(4)])


def exchanged(x, axes, count):
    parts = x.reshape(count, x.shape[0] // count, *x.shape[1:])
    return lax.all_to_all(parts, axes, split_axis=0, concat_axis=0, tiled=True).reshape(x.shape)


def body(
    mid_rows,
    cotangent,
    route_experts,
    route_weights,
    gate_weight,
    up_weight,
    down_weight,
    out_weight,
    queries,
    key_rows,
    value_rows,
    log_decay,
):
    return layer(
        mid_rows, cotangent, route_experts, route_weights, gate_weight[0], up_weight[0], down_weight[0],
        out_weight, queries, key_rows, value_rows, log_decay,
    )


def layer(
    mid_rows, cotangent, route_experts, route_weights, gate, up, down,
    out_weight, queries, key_rows, value_rows, log_decay,
):
    core = lax.axis_index("tp").astype(jnp.int32).reshape(1)
    place = jnp.stack([lax.axis_index(n).astype(jnp.int32) for n in ("tp", *SP)])
    ids, wts = route_experts.T, route_weights.T
    mid2, cot2, ids2, wts2 = swapped(mid_rows), swapped(cotangent), swapped(ids), swapped(wts)
    dma = pltpu.SemaphoreType.DMA
    state_msg = call(
        state_kernel, fast((512, SW), bf16), (key_rows, value_rows, log_decay), "ppp", flops=1 << 28
    )
    send, pick = call(
        pack_kernel,
        (far_out((512, MSG), bf16), far_out((512, 2 * ROWS), bf16)),
        (core, ids, ids2, wts, wts2, mid_rows, mid2, cotangent, cot2, state_msg),
        "spnpnfnfnn",
        [pltpu.VMEM((2 * ROWS, D), bf16), pltpu.VMEM((512, D), bf16), pltpu.VMEM((512, 2 * ROWS), bf16), dma((8,))],
        flops=1 << 28,
        manual=(0, 1),
    )
    got = exchanged(send, SP, NDEV)
    keys, values, states = (TOK, 512), (TOK, HALF), (512, DV)
    inner, q_abs, key_end, to_end, state_local = call(
        prior_kernel,
        [far_out(d, f32) for d in (values, keys, keys, keys, states)],
        (queries, key_rows, value_rows, log_decay),
        "pppp",
        flops=1 << 29,
    )
    theirs = swapped(got)

    def scanned(msgs, reverse):
        return call(
            functools.partial(scan_kernel, reverse=reverse),
            far_out(states, bf16),
            (*msgs, got),
            "n" * len(msgs) + "f",
            [pltpu.VMEM((512, SW), bf16)] + [pltpu.VMEM(states, f32)] * 3 + [dma((1,))],
            flops=1 << 26,
        )

    state_out = scanned((), False)
    state_in = exchanged(state_out, SP, NDEV)
    gate, up, down = call(
        load_kernel,
        [fast(w.shape, bf16) for w in (gate, up, down)],
        (gate, up, down),
        "fff",
        [dma((3,))],
        flops=1 << 29,
        limit=2,
        manual=(),
    )
    hid = (512, HID)
    keep, give, hidden, back_gate, back_up = call(
        expert_kernel,
        (fast((512, HALF), bf16), fast((512, HALF), bf16)) + (far_out(hid, bf16),) * 3,
        (core, got, theirs, gate, up, down),
        "sffnnn",
        [pltpu.VMEM((512, D), bf16)] * 2 + [pltpu.VMEM(hid, bf16)] * 3 + [dma((5,))],
        flops=6 << 30,
        limit=24,
        manual=(2, 3, 4),
    )
    back = swapped(give)
    summed = call(return_kernel, far_out((512, HALF), bf16), (keep, back), "nn", flops=1 << 20)
    ret = exchanged(summed, SP, NDEV)
    normed, inv, rounded, state_end = call(
        forward_kernel,
        (far_out(values, f32), far_out(keys, f32), far_out(values, bf16), far_out(states, f32)),
        (inner, q_abs, state_in, state_local, log_decay),
        "ppppp",
        flops=1 << 28,
    )
    normeds = [rounded] + [turned(rounded, "sp_0", n) for n in range(1, 4)]
    token_mine = call(
        combine_kernel,
        fast(values, bf16),
        (core, pick, ret, cotangent, cot2),
        "spnpp",
        flops=1 << 26,
    )
    token_theirs = swapped(token_mine)
    (near_weight,) = call(
        load_kernel,
        [fast(out_weight.shape, bf16)],
        (out_weight,),
        "f",
        [dma((1,))],
        flops=1 << 29,
        limit=2,
    )
    back_msg, braw, *columns = call(
        mixer_kernel,
        (far_out(states, bf16), far_out(values, f32)) + (far_out((TOK, HID), bf16),) * 4,
        (place, token_mine, token_theirs, near_weight, q_abs, normed, inv),
        "snnnppp",
        flops=1 << 30,
    )
    back_got = exchanged(back_msg, SP, NDEV)
    columns = columns[:1] + [turned(columns[n], "sp_0", n) for n in range(1, 4)]
    state_back = scanned((back_got,), True)
    future = exchanged(state_back, SP, NDEV)
    query_out, dk_part, dv_part, dd_part = call(
        local_kernel,
        (far_out(keys, bf16), far_out(keys, f32), far_out(values, f32), far_out(keys, f32)),
        (queries, key_rows, value_rows, log_decay, state_in, braw),
        "pppppp",
        flops=1 << 30,
    )
    outer = call(outer_kernel, far_out((512, HALF), bf16), (*columns, *normeds), "pnnnpppp", flops=1 << 29)
    terms = lax.all_to_all(
        outer.reshape(16, 32, HALF), ("sp_1", "sp_2"), split_axis=0, concat_axis=0, tiled=True
    )
    key_out, value_out, decay_out = call(
        final_kernel,
        (far_out(keys, bf16), far_out(values, bf16), far_out(keys, f32)),
        (key_rows, value_rows, key_end, to_end, state_end, future, dk_part, dv_part, dd_part),
        "pppppnppp",
        flops=1 << 29,
    )
    gate_total, up_total, down_total = call(
        grads_kernel,
        (far_out((D, HID), bf16), far_out((D, HID), bf16), far_out((HID, D), bf16)),
        (core, got, theirs, hidden, back_gate, back_up),
        "sffppp",
        [pltpu.VMEM((512, D), bf16)] * 2 + [dma((2,))],
        flops=3 << 30,
        limit=28,
    )
    out_total = call(total_kernel, far_out((32, HALF), f32), (terms,), "n", flops=1 << 20)
    totals = (gate_total[None], up_total[None], down_total[None])
    return (*totals, out_total, query_out, key_out, value_out, decay_out)


def solution(mesh):
    split = Mesh(mesh.devices.reshape(4, 4, 4, mesh.shape["tp"]), ("sp_0", "sp_1", "sp_2", "tp"))
    placed = (
        P(SP_TP, None),
        P(SP_TP, None),
        P(SP_TP, None),
        P(SP_TP, None),
        P(SP, None, "tp"),
        P(SP, None, "tp"),
        P(SP, "tp", None),
        P(None, "tp"),
        P(SP, "tp"),
        P(SP, "tp"),
        P(SP, "tp"),
        P(SP, "tp"),
    )
    return jax.shard_map(
        body,
        mesh=split,
        in_specs=placed,
        out_specs=(
            P(SP, None, "tp"),
            P(SP, None, "tp"),
            P(SP, "tp", None),
            P(SP, "tp"),
            P(SP, "tp"),
            P(SP, "tp"),
            P(SP, "tp"),
            P(SP, "tp"),
        ),
        check_vma=False,
    )
```

time: 210 us -> 194 us (0.924)
  blocking collectives: 90.9 us -> 46.2 us
  starting transfers between devices: 13.1 us -> 43.3 us
  local copies, waits for them, and re-layouts: 4.04 us -> 18 us
  matrix products: 8.93 us -> 0 us
  Pallas kernels: 56.7 us -> 51 us
  other arithmetic: 2.21 us -> 0.08 us
    all_to_all x3 -> x1, blocking collectives: 90.9 us -> 46.2 us  [exchanged(): lax.all_to_all(parts, axes, split_axis=0, concat_axis=0, tiled=True)]
    all_to_all x1 -> x4, starting transfers between devices: 4.68 us -> 24.1 us  [exchanged(): lax.all_to_all(parts, axes, split_axis=0, concat_axis=0, tiled=True)]
    all_to_all x2 -> x1, waiting for transfers between devices: 18.3 us -> 0.01 us  [layer(): lax.all_to_all(outer.reshape(16, 32, HALF), ('sp_1', 'sp_2'), split_axis=...]
    all_to_all x1 -> x4, waiting for transfers between devices: 6.94 us -> 23.8 us  [exchanged(): lax.all_to_all(parts, axes, split_axis=0, concat_axis=0, tiled=True)]
    unnamed x28 -> x70, local copies, waits for them, and re-layouts: 3.94 us -> 18 us
    ppermute x0 -> x6, starting transfers between devices: none -> 11.8 us  [turned(): return lax.ppermute(x, axis, [(n, (n + shift) % 4) for n in range(4)])]
    dot_general x3 -> x0, matrix products: 8.93 us -> none  [dot(): lax.dot_general(a, b, (((ca,), (cb,)), ((), ())), precision=lax.Precision...]
    ppermute x0 -> x6, waiting for transfers between devices: none -> 6.04 us  [turned(): return lax.ppermute(x, axis, [(n, (n + shift) % 4) for n in range(4)])]
  transfers between devices with their start and end apart: 9 -> 18, of which waited for: 5 -> 7; matrix products, arithmetic and copies ran while one was open for 5% -> 0% of each run, Pallas kernels for 11% -> 18%
where the time goes in v1:
time: 194 us; the launch traced here: 193 us
  Pallas kernels  51 us (26%)
  blocking collectives  46.2 us (24%)
  starting transfers between devices  43.3 us (22%)
  waiting for transfers between devices  33.3 us (17%)
  local copies, waits for them, and re-layouts  18 us (9%)
    pallas_call x17, Pallas kernels, call(): pl.pallas_call(kernel, out_shape=out_shape, in_specs=[specs.get(k, vmem)...  51 us
    all_to_all x1, blocking collectives, exchanged(): lax.all_to_all(parts, axes, split_axis=0, concat_axis=0, tiled=True)  46.2 us
    all_to_all x4, starting transfers between devices, exchanged(): lax.all_to_all(parts, axes, split_axis=0, concat_axis=0, tiled=True)  24.1 us
    all_to_all x4, waiting for transfers between devices, exchanged(): lax.all_to_all(parts, axes, split_axis=0, concat_axis=0, tiled=True)  23.8 us
    unnamed x70, local copies, waits for them, and re-layouts  18 us
    ppermute x6, starting transfers between devices, turned(): return lax.ppermute(x, axis, [(n, (n + shift) % 4) for n in range(4)])  11.8 us
    all_to_all x1, starting transfers between devices, layer(): lax.all_to_all(outer.reshape(16, 32, HALF), ('sp_1', 'sp_2'), split_axis=...  6.09 us
    ppermute x6, waiting for transfers between devices, turned(): return lax.ppermute(x, axis, [(n, (n + shift) % 4) for n in range(4)])  6.04 us
  transfers between devices with their start and end apart: 18, of which 7 were waited for; matrix products, arithmetic and copies ran while one was open for 0% of the time, Pallas kernels for 18%

profile of v1, /device:TPU:0, one launch (start us, length us, event | category | flops | bytes accessed | tf_op | source)
XLA Modules:
  0.0 193.0 jit_solution(14798495114583767545)
XLA Ops:
  7.2 2.7 %shard_map.180 = (bf16[512,2432]{1,0:T(8,128)(2,1)}, bf16[512,128]{1,0:T(8,128)(2,1)}) custom-call(s32[1]{0:T(128)} %bitcast.core_ref, s32[2,64]{1,0:T(2,128)S(1)} %bitcast.29, s32[2,64]{1,0:T(2,128)S(1)} %collective-permute-done.ids2_ref, f32[2,64]{1,0:T(2,128)S(1)} %bitcast.31, f32[2,64]{1,0:T(2,128)S(1)} %collective-permute-done.1.wts2_ref, ...), custom_call_target="tpu_custom_call" | custom-call | flops 268435456 | bytes 1048576 | tf_op jit(solution)/shard_map/pallas_call | solution.py:64
  9.9 46.2 %all_to_all.30 = bf16[64,8,2432]{2,1,0:T(8,128)(2,1)S(1)} all-to-all(bf16[64,8,2432]{2,1,0:T(8,128)(2,1)} %bitcast.39), channel_id=1, replica_groups=mesh['sp_0'=4,'sp_1'=4,'sp_2'=4,'tp'=2] {'sp_0','sp_1','sp_2'}, dimensions={0} | all-to-all | bytes 4980736 | tf_op jit(solution)/shard_map/all_to_all | solution.py:423
  56.2 3.8 %shard_map.181 = (bf16[2048,512]{1,0:T(8,128)(2,1)S(1)}, bf16[2048,512]{1,0:T(8,128)(2,1)S(1)}, bf16[512,2048]{1,0:T(8,128)(2,1)S(1)}) custom-call(bf16[2048,512]{1,0:T(8,128)(2,1)} %bitcast.40, bf16[2048,512]{1,0:T(8,128)(2,1)} %bitcast.41, bf16[512,2048]{1,0:T(8,128)(2,1)} %bitcast.42), custom_call_target="tpu_custom_call" | custom-call | flops 536870912 | bytes 1048576 | tf_op jit(solution)/shard_map/pallas_call | solution.py:64
  62.4 7.7 %shard_map.182 = (bf16[512,1024]{1,0:T(8,128)(2,1)S(1)}, bf16[512,1024]{1,0:T(8,128)(2,1)S(1)}, bf16[512,512]{1,0:T(8,128)(2,1)}, bf16[512,512]{1,0:T(8,128)(2,1)}, bf16[512,512]{1,0:T(8,128)(2,1)}) custom-call(s32[1]{0:T(128)} %bitcast.core_ref, bf16[512,2432]{1,0:T(8,128)(2,1)} %bitcast.33, bf16[512,2432]{1,0:T(8,128)(2,1)} %copy-done.31, ...), custom_call_target="tpu_custom_call" | custom-call | flops 6442450944 | bytes 1048576 | tf_op jit(solution)/shard_map/pallas_call | solution.py:64
  70.3 2.5 %collective-permute-done.5.got_ref = bf16[512,1024]{1,0:T(8,128)(2,1)S(1)} collective-permute-done((bf16[512,1024]{1,0:T(8,128)(2,1)S(1)}, bf16[512,1024]{1,0:T(8,128)(2,1)S(1)}, u32[]{:S(2)}, u32[]{:S(2)}) %collective-permute-start.5) | collective-permute-done | bytes 1048608 | tf_op jit(solution)/shard_map/ppermute | solution.py:414
  74.0 5.3 %all-to-all-start.1 = ((bf16[64,8,1024]{2,1,0:T(8,128)(2,1)}), bf16[64,8,1024]{2,1,0:T(8,128)(2,1)S(1)}, u32[]{:S(2)}, u32[]{:S(2)}) async-start(bf16[64,8,1024]{2,1,0:T(8,128)(2,1)} %bitcast.37), calls=%async_computation.1 | async-start | bytes 2097152 | tf_op jit(solution)/shard_map/all_to_all | solution.py:423
  81.4 17.1 %all-to-all-done.1 = bf16[64,8,1024]{2,1,0:T(8,128)(2,1)S(1)} async-done(((bf16[64,8,1024]{2,1,0:T(8,128)(2,1)}), bf16[64,8,1024]{2,1,0:T(8,128)(2,1)S(1)}, u32[]{:S(2)}, u32[]{:S(2)}) %all-to-all-start.1) | async-done | bytes 1048608 | tf_op jit(solution)/shard_map/all_to_all | solution.py:423
  98.6 4.9 %all-to-all-start.2 = ((bf16[64,8,256]{2,1,0:T(8,128)(2,1)}), bf16[64,8,256]{2,1,0:T(8,128)(2,1)S(1)}, u32[]{:S(2)}, u32[]{:S(2)}) async-start(bf16[64,8,256]{2,1,0:T(8,128)(2,1)} %bitcast.44), calls=%async_computation.2 | async-start | bytes 524288 | tf_op jit(solution)/shard_map/all_to_all | solution.py:423
  104.2 4.0 %shard_map.187 = (f32[128,1024]{1,0:T(8,128)}, f32[128,512]{1,0:T(8,128)}, f32[128,512]{1,0:T(8,128)}, f32[128,512]{1,0:T(8,128)}, f32[512,256]{1,0:T(8,128)}) custom-call(bf16[128,512]{1,0:T(8,128)(2,1)S(1)} %copy-done.26, bf16[128,512]{1,0:T(8,128)(2,1)S(1)} %copy-done.14, bf16[128,1024]{1,0:T(8,128)(2,1)S(1)} %copy-done.7, f32[128,512]{1,0:T(8,128)S(1)} %copy-done.5), custom_call_target="tpu_custom_call" | custom-call | flops 536870912 | bytes 1048576 | tf_op jit(solution)/shard_map/pallas_call | solution.py:64
  108.2 2.3 %shard_map.186.w_ref = bf16[2048,1024]{1,0:T(8,128)(2,1)S(1)} custom-call(bf16[2048,1024]{1,0:T(8,128)(2,1)} %refs_0_.1), custom_call_target="tpu_custom_call" | custom-call | flops 536870912 | bytes 1048576 | tf_op jit(solution)/shard_map/pallas_call | solution.py:64
  115.9 2.2 %copy-done.1 = bf16[2048,1024]{1,0:T(8,128)(2,1)S(1)} copy-done((bf16[2048,1024]{1,0:T(8,128)(2,1)S(1)}, bf16[2048,1024]{1,0:T(8,128)(2,1)}, u32[]{:S(2)}) %copy-start.1) | copy-done | bytes 4194328
  120.1 3.9 %shard_map.190 = (bf16[512,256]{1,0:T(8,128)(2,1)}, f32[128,1024]{1,0:T(8,128)}, bf16[128,512]{1,0:T(8,128)(2,1)}, bf16[128,512]{1,0:T(8,128)(2,1)}, bf16[128,512]{1,0:T(8,128)(2,1)}, /*index=5*/bf16[128,512]{1,0:T(8,128)(2,1)}) custom-call(s32[4]{0:T(128)S(1)} %pad_add_fusion.place_ref, bf16[128,1024]{1,0:T(8,128)(2,1)S(1)} %shard_map.185.mine_ref, ...), custom_call_target="tpu_custom_call" | custom-call | flops 1073741824 | bytes 1048576 | tf_op jit(solution)/shard_map/pallas_call | solution.py:64
  124.0 9.0 %all-to-all-start.4 = ((bf16[64,8,256]{2,1,0:T(8,128)(2,1)}), bf16[64,8,256]{2,1,0:T(8,128)(2,1)S(1)}, u32[]{:S(2)}, u32[]{:S(2)}) async-start(bf16[64,8,256]{2,1,0:T(8,128)(2,1)} %bitcast.45), calls=%async_computation.4 | async-start | bytes 524288 | tf_op jit(solution)/shard_map/all_to_all | solution.py:423
  134.6 2.9 %collective-permute-start.11 = (bf16[128,1024]{1,0:T(8,128)(2,1)S(1)}, bf16[128,1024]{1,0:T(8,128)(2,1)S(1)}, u32[]{:S(2)}, u32[]{:S(2)}) collective-permute-start(bf16[128,1024]{1,0:T(8,128)(2,1)S(1)} %copy-done.15), channel_id=1, source_target_pairs={{0,64},{32,96},{64,0},{96,32},{1,65},{33,97},{65,1},{97,33},{2,66}... | collective-permute-start | bytes 786440 | tf_op jit(solution)/shard_map/ppermute | solution.py:418
  138.9 5.3 %all-to-all-done.4 = bf16[64,8,256]{2,1,0:T(8,128)(2,1)S(1)} async-done(((bf16[64,8,256]{2,1,0:T(8,128)(2,1)}), bf16[64,8,256]{2,1,0:T(8,128)(2,1)S(1)}, u32[]{:S(2)}, u32[]{:S(2)}) %all-to-all-start.4) | async-done | bytes 262176 | tf_op jit(solution)/shard_map/all_to_all | solution.py:423
  146.1 4.9 %all-to-all-start.5 = ((bf16[64,8,256]{2,1,0:T(8,128)(2,1)}), bf16[64,8,256]{2,1,0:T(8,128)(2,1)S(1)}, u32[]{:S(2)}, u32[]{:S(2)}) async-start(bf16[64,8,256]{2,1,0:T(8,128)(2,1)} %bitcast.43), calls=%async_computation.5 | async-start | bytes 524288 | tf_op jit(solution)/shard_map/all_to_all | solution.py:423
  152.7 2.9 %collective-permute-start.8 = (bf16[128,512]{1,0:T(8,128)(2,1)S(1)}, bf16[128,512]{1,0:T(8,128)(2,1)S(1)}, u32[]{:S(2)}, u32[]{:S(2)}) collective-permute-start(bf16[128,512]{1,0:T(8,128)(2,1)S(1)} %copy-done.33), channel_id=1, source_target_pairs={{0,64},{32,96},{64,0},{96,32},{1,65},{33,97},{65,1},{97,33},{2,66}... | collective-permute-start | bytes 393224 | tf_op jit(solution)/shard_map/ppermute | solution.py:418
  156.9 3.4 %collective-permute-done.7.refs_1_ = bf16[128,512]{1,0:T(8,128)(2,1)S(1)} collective-permute-done((bf16[128,512]{1,0:T(8,128)(2,1)S(1)}, bf16[128,512]{1,0:T(8,128)(2,1)S(1)}, u32[]{:S(2)}, u32[]{:S(2)}) %collective-permute-start.7) | collective-permute-done | bytes 131104 | tf_op jit(solution)/shard_map/ppermute | solution.py:418
  160.4 2.6 %collective-permute-done.8.refs_2_ = bf16[128,512]{1,0:T(8,128)(2,1)S(1)} collective-permute-done((bf16[128,512]{1,0:T(8,128)(2,1)S(1)}, bf16[128,512]{1,0:T(8,128)(2,1)S(1)}, u32[]{:S(2)}, u32[]{:S(2)}) %collective-permute-start.8) | collective-permute-done | bytes 131104 | tf_op jit(solution)/shard_map/ppermute | solution.py:418
  163.0 2.3 %shard_map.191 = bf16[512,1024]{1,0:T(8,128)(2,1)} custom-call(bf16[128,512]{1,0:T(8,128)(2,1)S(1)} %copy-done.21, bf16[128,512]{1,0:T(8,128)(2,1)S(1)} %collective-permute-done.7.refs_1_, bf16[128,512]{1,0:T(8,128)(2,1)S(1)} %collective-permute-done.8.refs_2_, bf16[128,512]{1,0:T(8,128)(2,1)S(1)} %collective-permute-done.9.refs_3_, ...), custom_call_target="tpu_custom_call" | custom-call | flops 536870912 | bytes 1048576 | tf_op jit(solution)/shard_map/pallas_call | solution.py:64
  165.2 6.1 %all-to-all-start.3 = ((bf16[16,32,1024]{2,1,0:T(8,128)(2,1)}), bf16[16,32,1024]{2,1,0:T(8,128)(2,1)S(1)}, u32[]{:S(2)}, u32[]{:S(2)}) async-start(bf16[16,32,1024]{2,1,0:T(8,128)(2,1)} %bitcast.38), calls=%async_computation.3 | async-start | bytes 2097152 | tf_op jit(solution)/shard_map/all_to_all | solution.py:558
  174.5 8.5 %shard_map.183 = (bf16[2048,512]{1,0:T(8,128)(2,1)}, bf16[2048,512]{1,0:T(8,128)(2,1)}, bf16[512,2048]{1,0:T(8,128)(2,1)}) custom-call(s32[1]{0:T(128)} %bitcast.core_ref, bf16[512,2432]{1,0:T(8,128)(2,1)} %bitcast.36, bf16[512,2432]{1,0:T(8,128)(2,1)} %copy-done.31, bf16[512,512]{1,0:T(8,128)(2,1)S(1)} %copy-done.27, bf16[512,512]{1,0:T(8,128)(2,1)S(1)} %copy-done.28, ...), custom_call_target="tpu_custom_call" | custom-call | flops 3221225472 | bytes 1048576 | tf_op jit(solution)/shard_map/pallas_call | solution.py:64
  183.1 4.1 %shard_map.193 = (bf16[128,512]{1,0:T(8,128)(2,1)}, f32[128,512]{1,0:T(8,128)}, f32[128,1024]{1,0:T(8,128)}, f32[128,512]{1,0:T(8,128)}) custom-call(bf16[128,512]{1,0:T(8,128)(2,1)S(1)} %copy-done.26, bf16[128,512]{1,0:T(8,128)(2,1)S(1)} %copy-done.14, bf16[128,1024]{1,0:T(8,128)(2,1)S(1)} %copy-done.7, f32[128,512]{1,0:T(8,128)S(1)} %copy-done.5, ...), custom_call_target="tpu_custom_call" | custom-call | flops 1073741824 | bytes 1048576 | tf_op jit(solution)/shard_map/pallas_call | solution.py:64
  190.1 2.1 %shard_map.195 = (bf16[128,512]{1,0:T(8,128)(2,1)}, bf16[128,1024]{1,0:T(8,128)(2,1)}, f32[128,512]{1,0:T(8,128)}) custom-call(bf16[128,512]{1,0:T(8,128)(2,1)S(1)} %copy-done.14, bf16[128,1024]{1,0:T(8,128)(2,1)S(1)} %copy-done.7, f32[128,512]{1,0:T(8,128)S(1)} %copy-done.17, f32[128,512]{1,0:T(8,128)S(1)} %copy-done.18, f32[512,256]{1,0:T(8,128)S(1)} %copy-done.11, ...), custom_call_target="tpu_custom_call" | custom-call | flops 536870912 | bytes 1048576 | tf_op jit(solution)/shard_map/pallas_call | solution.py:64
  (101 shorter events, 35.2 us)
Async XLA Ops:
  0.6 5.2 %collective-permute-start.3 = (bf16[64,2048]{1,0:T(8,128)(2,1)}, bf16[64,2048]{1,0:T(8,128)(2,1)S(1)}, u32[]{:S(2)}, u32[]{:S(2)}) collective-permute-start(bf16[64,2048]{1,0:T(8,128)(2,1)} %cot_ref.3), channel_id=1, source_target_pairs={{0,1},{1,0},{2,3},{3,2},{4,5},{5,4},{6,7},{7,6},{8,9},{9,8},{10,11... | collective-permute-start | bytes 786440 | tf_op jit(solution)/shard_map/ppermute | solution.py:414
  0.7 5.1 %collective-permute-start.2 = (bf16[64,2048]{1,0:T(8,128)(2,1)}, bf16[64,2048]{1,0:T(8,128)(2,1)S(1)}, u32[]{:S(2)}, u32[]{:S(2)}) collective-permute-start(bf16[64,2048]{1,0:T(8,128)(2,1)} %mid_ref.1), channel_id=1, source_target_pairs={{0,1},{1,0},{2,3},{3,2},{4,5},{5,4},{6,7},{7,6},{8,9},{9,8},{10,11... | collective-permute-start | bytes 786440 | tf_op jit(solution)/shard_map/ppermute | solution.py:414
  1.2 4.6 %collective-permute-start = (s32[2,64]{1,0:T(2,128)}, s32[2,64]{1,0:T(2,128)S(1)}, u32[]{:S(2)}, u32[]{:S(2)}) collective-permute-start(s32[2,64]{1,0:T(2,128)} %bitcast.28), channel_id=1, source_target_pairs={{0,1},{1,0},{2,3},{3,2},{4,5},{5,4},{6,7},{7,6},{8,9},{9,8},{10,11... | collective-permute-start | bytes 1544 | tf_op jit(solution)/shard_map/ppermute | solution.py:414
  1.3 4.5 %collective-permute-start.1 = (f32[2,64]{1,0:T(2,128)}, f32[2,64]{1,0:T(2,128)S(1)}, u32[]{:S(2)}, u32[]{:S(2)}) collective-permute-start(f32[2,64]{1,0:T(2,128)} %bitcast.30), channel_id=1, source_target_pairs={{0,1},{1,0},{2,3},{3,2},{4,5},{5,4},{6,7},{7,6},{8,9},{9,8},{10,11... | collective-permute-start | bytes 1544 | tf_op jit(solution)/shard_map/ppermute | solution.py:414
  56.2 4.7 %collective-permute-start.4 = (bf16[512,2432]{1,0:T(8,128)(2,1)S(1)}, bf16[512,2432]{1,0:T(8,128)(2,1)S(1)}, u32[]{:S(2)}, u32[]{:S(2)}) collective-permute-start(bf16[512,2432]{1,0:T(8,128)(2,1)S(1)} %bitcast.32), channel_id=1, source_target_pairs={{0,1},{1,0},{2,3},{3,2},{4,5},{5,4},{6,7},{7,6},{8,9},{9,8},{10,11... | collective-permute-start | bytes 7471112 | tf_op jit(solution)/shard_map/ppermute | solution.py:414
  70.1 2.7 %collective-permute-start.5 = (bf16[512,1024]{1,0:T(8,128)(2,1)S(1)}, bf16[512,1024]{1,0:T(8,128)(2,1)S(1)}, u32[]{:S(2)}, u32[]{:S(2)}) collective-permute-start(bf16[512,1024]{1,0:T(8,128)(2,1)S(1)} %get-tuple-element.55), channel_id=1, source_target_pairs={{0,1},{1,0},{2,3},{3,2},{4,5},{5,4},{6,7},{7,6},{8,9},{9,8},{10,11... | collective-permute-start | bytes 3145736 | tf_op jit(solution)/shard_map/ppermute | solution.py:414
  74.0 24.5 %all-to-all-start.1 = ((bf16[64,8,1024]{2,1,0:T(8,128)(2,1)}), bf16[64,8,1024]{2,1,0:T(8,128)(2,1)S(1)}, u32[]{:S(2)}, u32[]{:S(2)}) async-start(bf16[64,8,1024]{2,1,0:T(8,128)(2,1)} %bitcast.37), calls=%async_computation.1 | async-start | bytes 2097152 | tf_op jit(solution)/shard_map/all_to_all | solution.py:423
  79.4 24.7 %copy-start.5 = (f32[128,512]{1,0:T(8,128)S(1)}, f32[128,512]{1,0:T(8,128)}, u32[]{:S(2)}) copy-start(f32[128,512]{1,0:T(8,128)} %a_ref.7) | copy-start | bytes 786436
  79.4 24.7 %copy-start.7 = (bf16[128,1024]{1,0:T(8,128)(2,1)S(1)}, bf16[128,1024]{1,0:T(8,128)(2,1)}, u32[]{:S(2)}) copy-start(bf16[128,1024]{1,0:T(8,128)(2,1)} %v_ref.7) | copy-start | bytes 786436
  98.6 15.4 %all-to-all-start.2 = ((bf16[64,8,256]{2,1,0:T(8,128)(2,1)}), bf16[64,8,256]{2,1,0:T(8,128)(2,1)S(1)}, u32[]{:S(2)}, u32[]{:S(2)}) async-start(bf16[64,8,256]{2,1,0:T(8,128)(2,1)} %bitcast.44), calls=%async_computation.2 | async-start | bytes 524288 | tf_op jit(solution)/shard_map/all_to_all | solution.py:423
  104.0 11.9 %collective-permute-start.6 = (bf16[128,1024]{1,0:T(8,128)(2,1)S(1)}, bf16[128,1024]{1,0:T(8,128)(2,1)S(1)}, u32[]{:S(2)}, u32[]{:S(2)}) collective-permute-start(bf16[128,1024]{1,0:T(8,128)(2,1)S(1)} %shard_map.185.mine_ref), channel_id=1, source_target_pairs={{0,1},{1,0},{2,3},{3,2},{4,5},{5,4},{6,7},{7,6},{8,9},{9,8},{10,11... | collective-permute-start | bytes 786440 | tf_op jit(solution)/shard_map/ppermute | solution.py:414
  124.0 27.1 %copy-start.34 = (bf16[128,512]{1,0:T(8,128)(2,1)S(1)}, bf16[128,512]{1,0:T(8,128)(2,1)}, u32[]{:S(2)}) copy-start(bf16[128,512]{1,0:T(8,128)(2,1)} %get-tuple-element.62) | copy-start | bytes 393220
  124.0 28.7 %copy-start.33 = (bf16[128,512]{1,0:T(8,128)(2,1)S(1)}, bf16[128,512]{1,0:T(8,128)(2,1)}, u32[]{:S(2)}) copy-start(bf16[128,512]{1,0:T(8,128)(2,1)} %get-tuple-element.63) | copy-start | bytes 393220
  124.0 31.6 %copy-start.32 = (bf16[128,512]{1,0:T(8,128)(2,1)S(1)}, bf16[128,512]{1,0:T(8,128)(2,1)}, u32[]{:S(2)}) copy-start(bf16[128,512]{1,0:T(8,128)(2,1)} %get-tuple-element.64) | copy-start | bytes 393220
  124.0 39.0 %copy-start.21 = (bf16[128,512]{1,0:T(8,128)(2,1)S(1)}, bf16[128,512]{1,0:T(8,128)(2,1)}, u32[]{:S(2)}) copy-start(bf16[128,512]{1,0:T(8,128)(2,1)} %get-tuple-element.61.refs_0_) | copy-start | bytes 393220
  124.0 20.2 %all-to-all-start.4 = ((bf16[64,8,256]{2,1,0:T(8,128)(2,1)}), bf16[64,8,256]{2,1,0:T(8,128)(2,1)S(1)}, u32[]{:S(2)}, u32[]{:S(2)}) async-start(bf16[64,8,256]{2,1,0:T(8,128)(2,1)} %bitcast.45), calls=%async_computation.4 | async-start | bytes 524288 | tf_op jit(solution)/shard_map/all_to_all | solution.py:423
  133.0 22.6 %collective-permute-start.10 = (bf16[128,1024]{1,0:T(8,128)(2,1)S(1)}, bf16[128,1024]{1,0:T(8,128)(2,1)S(1)}, u32[]{:S(2)}, u32[]{:S(2)}) collective-permute-start(bf16[128,1024]{1,0:T(8,128)(2,1)S(1)} %copy-done.15), channel_id=1, source_target_pairs={{0,32},{32,64},{64,96},{96,0},{1,33},{33,65},{65,97},{97,1},{2,34}... | collective-permute-start | bytes 786440 | tf_op jit(solution)/shard_map/ppermute | solution.py:418
  134.6 22.3 %collective-permute-start.11 = (bf16[128,1024]{1,0:T(8,128)(2,1)S(1)}, bf16[128,1024]{1,0:T(8,128)(2,1)S(1)}, u32[]{:S(2)}, u32[]{:S(2)}) collective-permute-start(bf16[128,1024]{1,0:T(8,128)(2,1)S(1)} %copy-done.15), channel_id=1, source_target_pairs={{0,64},{32,96},{64,0},{96,32},{1,65},{33,97},{65,1},{97,33},{2,66}... | collective-permute-start | bytes 786440 | tf_op jit(solution)/shard_map/ppermute | solution.py:418
  137.5 19.4 %collective-permute-start.12 = (bf16[128,1024]{1,0:T(8,128)(2,1)S(1)}, bf16[128,1024]{1,0:T(8,128)(2,1)S(1)}, u32[]{:S(2)}, u32[]{:S(2)}) collective-permute-start(bf16[128,1024]{1,0:T(8,128)(2,1)S(1)} %copy-done.15), channel_id=1, source_target_pairs={{0,96},{32,0},{64,32},{96,64},{1,97},{33,1},{65,33},{97,65},{2,98}... | collective-permute-start | bytes 786440 | tf_op jit(solution)/shard_map/ppermute | solution.py:418
  146.1 19.1 %all-to-all-start.5 = ((bf16[64,8,256]{2,1,0:T(8,128)(2,1)}), bf16[64,8,256]{2,1,0:T(8,128)(2,1)S(1)}, u32[]{:S(2)}, u32[]{:S(2)}) async-start(bf16[64,8,256]{2,1,0:T(8,128)(2,1)} %bitcast.43), calls=%async_computation.5 | async-start | bytes 524288 | tf_op jit(solution)/shard_map/all_to_all | solution.py:423
  151.0 9.3 %collective-permute-start.7 = (bf16[128,512]{1,0:T(8,128)(2,1)S(1)}, bf16[128,512]{1,0:T(8,128)(2,1)S(1)}, u32[]{:S(2)}, u32[]{:S(2)}) collective-permute-start(bf16[128,512]{1,0:T(8,128)(2,1)S(1)} %copy-done.34), channel_id=1, source_target_pairs={{0,32},{32,64},{64,96},{96,0},{1,33},{33,65},{65,97},{97,1},{2,34}... | collective-permute-start | bytes 393224 | tf_op jit(solution)/shard_map/ppermute | solution.py:418
  152.7 10.3 %collective-permute-start.8 = (bf16[128,512]{1,0:T(8,128)(2,1)S(1)}, bf16[128,512]{1,0:T(8,128)(2,1)S(1)}, u32[]{:S(2)}, u32[]{:S(2)}) collective-permute-start(bf16[128,512]{1,0:T(8,128)(2,1)S(1)} %copy-done.33), channel_id=1, source_target_pairs={{0,64},{32,96},{64,0},{96,32},{1,65},{33,97},{65,1},{97,33},{2,66}... | collective-permute-start | bytes 393224 | tf_op jit(solution)/shard_map/ppermute | solution.py:418
  155.6 7.4 %collective-permute-start.9 = (bf16[128,512]{1,0:T(8,128)(2,1)S(1)}, bf16[128,512]{1,0:T(8,128)(2,1)S(1)}, u32[]{:S(2)}, u32[]{:S(2)}) collective-permute-start(bf16[128,512]{1,0:T(8,128)(2,1)S(1)} %copy-done.32), channel_id=1, source_target_pairs={{0,96},{32,0},{64,32},{96,64},{1,97},{33,1},{65,33},{97,65},{2,98}... | collective-permute-start | bytes 393224 | tf_op jit(solution)/shard_map/ppermute | solution.py:418
  165.2 27.0 %all-to-all-start.3 = ((bf16[16,32,1024]{2,1,0:T(8,128)(2,1)}), bf16[16,32,1024]{2,1,0:T(8,128)(2,1)S(1)}, u32[]{:S(2)}, u32[]{:S(2)}) async-start(bf16[16,32,1024]{2,1,0:T(8,128)(2,1)} %bitcast.38), calls=%async_computation.3 | async-start | bytes 2097152 | tf_op jit(solution)/shard_map/all_to_all | solution.py:558
  (29 other events, 170.5 us)
